TPU v7x, 512 devices: a whole 4x8x8 slice. The times are simulated.
512 devices in a mesh: ep: 32 (over z, x), tp: 16 (over y, core).
Axes of the slice: x: 4, y: 8, z: 8, core: 2. Of those that a mesh axis runs over, the one named last changes fastest.
Arguments:
- queries: bfloat16 [8192, 2048], P('ep', 'tp'), may hold values from -9 to 9
- key_rows: bfloat16 [8192, 2048], P('ep', 'tp'), may hold values from -9 to 9
- values: bfloat16 [8192, 2048], P('ep', 'tp'), may hold values from -6 to 6
- second_scale: float32 [16], P('tp'), may hold values from 0.3 to 0.8
- head_gain: float32 [128], replicated, may hold values from 0.1 to 1.9
- out_weight: bfloat16 [2048, 2048], P(None, 'tp'), may hold values from -0.125 to 0.125
- routed_in: bfloat16 [8192, 2048], P('ep'), may hold values from -6 to 6
- routed_gain: float32 [2048], replicated, may hold values from 0.1 to 1.9
- expert_ids: int32 [8192, 2], P('ep'), may hold values from 0 to 31, all different within a row; in each aligned block of 256 rows (0 to 255, 256 to 511, ...) at most 32 rows name the same one
- group_logits: float32 [8192, 8], P('ep'), may hold values from -6 to 6
- inner_logits: float32 [8192, 2], P('ep'), may hold values from -6 to 6
- gate_weight: bfloat16 [32, 2048, 4096], P('ep', None, 'tp'), may hold values from -0.125 to 0.125
- up_weight: bfloat16 [32, 2048, 4096], P('ep', None, 'tp'), may hold values from -0.125 to 0.125
- down_weight: bfloat16 [32, 4096, 2048], P('ep', 'tp'), may hold values from -0.09375 to 0.09375
Outputs:
- mixer_out: bfloat16 [8192, 2048], P('ep', 'tp')
- routed_out: bfloat16 [8192, 2048], P('ep', 'tp')
Inputs may be any that keep to these rules, and one draw needn't show every extreme that they name: `expert_ids`: the two ids of a row differ. In the rows of one device (aligned blocks of 256 rows) no expert is named by more than 32 rows, a bound that some block reaches.
All inputs are finite; a program needn't handle non-finite values.
Results may differ from a plain program's by a relative error of at most 0.018.
Values may be sent and summed in bfloat16 or wider, within the bound.
A program may use at most 128 MiB of HBM per device.

v0:
```python
import math

import jax
import jax.numpy as jnp
from jax import lax
from jax.sharding import Mesh
from jax.sharding import PartitionSpec as P

GROUP_SIZE = 4
EP = ("ep_0", "ep_1")


EPSILON = 1e-05
LOWEST = -1e30


def whole_of(array, axes, dim):
    if not axes:
        return array
    nearer = lax.all_gather(array, axes[-1], axis=dim, tiled=True)
    return whole_of(nearer, axes[:-1], dim)


def token_mixer(queries, key_rows, values, second_scale, head_gain, out_weight):
    row_count = queries.shape[0]
    local_heads = second_scale.shape[0]
    qk_size = queries.shape[1] // (2 * local_heads)
    value_size = values.shape[1] // local_heads
    first_pos = lax.axis_index(EP) * row_count
    query_pos = first_pos + jnp.arange(row_count, dtype=jnp.int32)
    last_pos = first_pos + row_count - 1
    query_four = queries.reshape(row_count, local_heads, 2, qk_size)
    score_scale = qk_size ** (-0.5)
    initial = (
        jnp.full((row_count, local_heads, 2), LOWEST, jnp.float32),
        jnp.zeros((row_count, local_heads, 2), jnp.float32),
        jnp.zeros((row_count, local_heads, 2, value_size), jnp.float32),
    )
    state_now = initial
    key_piece = whole_of(key_rows, EP, 0)
    value_piece = whole_of(values, EP, 0)
    piece_count = key_piece.shape[0]
    block_width = math.gcd(piece_count, 512)
    blocks = piece_count // block_width
    key_blocks = key_piece.reshape(blocks, block_width, local_heads, 2, qk_size)
    value_blocks = value_piece.reshape(blocks, block_width, local_heads, value_size)

    def update(state_inner, block_index):
        key_start = block_index * block_width

        def attend(inner_state):
            running_max, denominator, weighted = inner_state
            scores = (
                jnp.einsum(
                    "qhmd,khmd->qhmk",
                    query_four,
                    key_blocks[block_index],
                    preferred_element_type=jnp.float32,
                )
                * score_scale
            )
            key_pos = key_start + jnp.arange(block_width, dtype=jnp.int32)
            visible = (query_pos[:, None] >= key_pos[None, :])[:, None, None, :]
            scores = jnp.where(visible, scores, LOWEST)
            new_max = jnp.maximum(running_max, jnp.max(scores, axis=-1))
            exp_terms = jnp.where(visible, jnp.exp(scores - new_max[..., None]), 0.0)
            factor = jnp.exp(running_max - new_max)
            denominator = denominator * factor + jnp.sum(exp_terms, axis=-1)
            weighted = weighted * factor[..., None] + jnp.einsum(
                "qhmk,khe->qhme",
                exp_terms.astype(jnp.bfloat16),
                value_blocks[block_index],
                preferred_element_type=jnp.float32,
            )
            return (new_max, denominator, weighted)

        return (
            lax.cond(key_start <= last_pos, attend, lambda inner_state: inner_state, state_inner),
            None,
        )

    state_now, _ = lax.scan(update, state_now, jnp.arange(blocks, dtype=jnp.int32))
    running_max, denominator, weighted = state_now
    mapped = weighted / denominator[..., None]
    difference = mapped[:, :, 0] - second_scale[None, :, None] * mapped[:, :, 1]
    inv_norm = lax.rsqrt(jnp.mean(difference * difference, axis=-1, keepdims=True) + EPSILON)
    head_out = (
        (difference * inv_norm * head_gain)
        .astype(jnp.bfloat16)
        .reshape(row_count, local_heads * value_size)
    )
    mixed = jnp.dot(
        lax.all_gather(head_out, "tp", axis=1, tiled=True),
        out_weight,
        preferred_element_type=jnp.float32,
    )
    return mixed.astype(jnp.bfloat16)


def expert_block(
    routed_in,
    routed_gain,
    expert_ids,
    group_logits,
    inner_logits,
    gate_weight,
    up_weight,
    down_weight,
):
    token_count = routed_in.shape[0]
    chosen = expert_ids.shape[1]
    ep_size = lax.axis_size(EP)
    capacity = 2 * chosen * token_count // ep_size
    source = routed_in.astype(jnp.float32)
    normed = (
        source
        * lax.rsqrt(jnp.mean(source * source, axis=-1, keepdims=True) + EPSILON)
        * routed_gain
    ).astype(jnp.bfloat16)
    flat_ids = expert_ids.reshape(-1)
    picked = (flat_ids[:, None] == jnp.arange(ep_size, dtype=jnp.int32)[None, :]).astype(jnp.int32)
    slot_index = jnp.sum(jnp.cumsum(picked, axis=0) * picked, axis=1) - 1
    place_index = flat_ids * capacity + slot_index
    owner_row = jnp.arange(token_count * chosen, dtype=jnp.int32) // chosen
    slot_rows = jnp.zeros((ep_size * capacity,), jnp.int32).at[place_index].set(owner_row)
    outgoing = normed[slot_rows].reshape(ep_size, capacity, normed.shape[1])
    gate_local = gate_weight[0]
    up_local = up_weight[0]
    down_local = down_weight[0]
    columns = outgoing.shape[2] // lax.axis_size("tp")
    own_columns = lax.dynamic_slice_in_dim(outgoing, lax.axis_index("tp") * columns, columns, 2)
    arrived = lax.all_to_all(own_columns, EP, split_axis=0, concat_axis=0, tiled=True)
    experts_arrived = lax.all_gather(arrived, "tp", axis=2, tiled=True)
    stacked = experts_arrived.reshape(-1, experts_arrived.shape[2])
    gate_act = jnp.dot(stacked, gate_local, preferred_element_type=jnp.float32)
    up_act = jnp.dot(stacked, up_local, preferred_element_type=jnp.float32)
    hidden = (jax.nn.silu(gate_act) * up_act).astype(jnp.bfloat16)
    partial_value = jnp.dot(hidden, down_local, preferred_element_type=jnp.float32)
    partial_value = partial_value.reshape(
        experts_arrived.shape[0], experts_arrived.shape[1], partial_value.shape[1]
    )
    answered = lax.psum_scatter(
        partial_value.astype(jnp.bfloat16), "tp", scatter_dimension=2, tiled=True
    )
    returned = lax.all_to_all(answered, EP, split_axis=0, concat_axis=0, tiled=True)
    pair_out = returned.reshape(ep_size * capacity, returned.shape[2])[place_index]
    pair_out = pair_out.reshape(token_count, chosen, returned.shape[2])
    group_prob = jax.nn.softmax(group_logits, axis=-1)
    member = (
        expert_ids[..., None] // GROUP_SIZE == jnp.arange(group_logits.shape[1], dtype=jnp.int32)
    ).astype(jnp.float32)
    group_pick = jnp.sum(group_prob[:, None, :] * member, axis=-1)
    route_weight = group_pick * jax.nn.softmax(inner_logits, axis=-1)
    return jnp.sum(route_weight[..., None] * pair_out.astype(jnp.float32), axis=1).astype(
        jnp.bfloat16
    )


def local(
    queries,
    key_rows,
    values,
    second_scale,
    head_gain,
    out_weight,
    routed_in,
    routed_gain,
    expert_ids,
    group_logits,
    inner_logits,
    gate_weight,
    up_weight,
    down_weight,
):
    mixer_out = token_mixer(queries, key_rows, values, second_scale, head_gain, out_weight)
    routed_out = expert_block(
        routed_in,
        routed_gain,
        expert_ids,
        group_logits,
        inner_logits,
        gate_weight,
        up_weight,
        down_weight,
    )
    return (mixer_out, routed_out)


def solution(mesh):
    finer = Mesh(mesh.devices.reshape(8, 4, mesh.shape["tp"]), ("ep_0", "ep_1", "tp"))
    placed = (
        P(EP, "tp"),
        P(EP, "tp"),
        P(EP, "tp"),
        P("tp"),
        P(),
        P(None, "tp"),
        P(EP, None),
        P(),
        P(EP, None),
        P(EP, None),
        P(EP, None),
        P(EP, None, "tp"),
        P(EP, None, "tp"),
        P(EP, "tp", None),
    )
    return jax.shard_map(
        local, mesh=finer, in_specs=placed, out_specs=(P(EP, "tp"), P(EP, "tp")), check_vma=False
    )
```

profile of v0, /device:TPU:1, one launch (start us, length us, event | category | flops | bytes accessed | tf_op | source)
XLA Modules:
  0.0 325.3 jit_solution(6230517476498490236)
XLA Ops:
  11.0 2.4 scatter_custom_fusion
  13.5 1.5 fusion.21
  15.0 1.5 fusion.23
  16.6 6.0 %gather_fusion = bf16[1024,2048]{1,0:T(8,128)(2,1)} fusion(bf16[256,2048]{1,0:T(8,128)(2,1)S(1)} %fusion.23, s32[1024]{0:T(1024)S(1)} %fusion.38), kind=kCustom, calls=%fused_computation | custom fusion | bytes 8392704 | tf_op jit(solution)/shard_map/gather | solution.py:126
  23.5 24.9 %all_to_all.10 = bf16[32,32,128]{2,1,0:T(8,128)(2,1)} all-to-all(bf16[32,32,128]{2,1,0:T(8,128)(2,1)S(1)} %constant_dynamic-slice_fusion), channel_id=1, replica_groups=mesh['ep_0'=8,'ep_1'=4,'tp'=16] {'ep_0','ep_1'}, dimensions={0} | all-to-all | bytes 524288 | tf_op jit(solution)/shard_map/all_to_all | solution.py:132
  48.6 10.7 %all_gather.18 = bf16[1024,128]{1,0:T(8,128)(2,1)} all-gather(bf16[256,128]{1,0:T(8,128)(2,1)S(1)} %copy-done.3), channel_id=1, replica_groups=mesh['ep_0'=8,'ep_1'=4,'tp'=16] {'ep_1'}, dimensions={0}, use_global_device_ids=true | all-gather | bytes 327680 | tf_op jit(solution)/shard_map/all_gather | solution.py:20
  59.4 11.1 %all_gather.20 = bf16[1024,128]{1,0:T(8,128)(2,1)} all-gather(bf16[256,128]{1,0:T(8,128)(2,1)S(1)} %copy-done.4), channel_id=1, replica_groups=mesh['ep_0'=8,'ep_1'=4,'tp'=16] {'ep_1'}, dimensions={0}, use_global_device_ids=true | all-gather | bytes 327680 | tf_op jit(solution)/shard_map/all_gather | solution.py:20
  70.6 28.3 %all-gather.11.cloned.1.call-done = bf16[32,32,2048]{2,1,0:T(8,128)(2,1)} async-done(((bf16[32,32,128]{2,1,0:T(8,128)(2,1)}), bf16[32,32,2048]{2,1,0:T(8,128)(2,1)}) %all-gather.11.cloned.1.call-update) | async-done | bytes 4194320 | tf_op jit(solution)/shard_map/all_gather | solution.py:133
  98.8 3.6 %fusion.27 = f32[1024,256]{1,0:T(8,128)S(1)} fusion(bf16[1024,2048]{1,0:T(8,128)(2,1)} %bitcast.107, bf16[1,2048,256]{2,1,0:T(8,128)(2,1)S(1)} %copy-done.9), kind=kOutput, calls=%fused_computation.42 | convolution fusion | flops 1073741824 | bytes 6291456 | tf_op jit(solution)/shard_map/dot_general | solution.py:135
  103.7 3.2 convolution_convert_fusion
  106.9 23.0 %copy.58 = bf16[32,32,2048]{1,0,2:T(8,128)(2,1)} copy(bf16[32,32,2048]{2,1,0:T(8,128)(2,1)} %convolution_convert_fusion) | data formatting | bytes 8388608
  130.0 23.3 %reshape.280 = bf16[2048,1024]{1,0:T(8,128)(2,1)} reshape(bf16[2048,32,32]{2,1,0:T(8,128)(2,1)} %bitcast.93) | data formatting | bytes 8388608
  154.9 8.2 %reshape.279 = bf16[16,512,1,2,64]{4,3,1,0,2:T(2,128)(2,1)} reshape(bf16[8192,128]{1,0:T(8,128)(2,1)} %all-gather.5.cloned.1.call-done) | data formatting | bytes 4194304 | tf_op jit(solution)/shard_map/reshape | solution.py:45
  163.1 9.1 %copy.48 = bf16[16,512,1,2,64]{1,4,3,2,0:T(8,128)(2,1)S(1)} copy(bf16[16,512,1,2,64]{4,3,1,0,2:T(2,128)(2,1)} %reshape.279) | data formatting | bytes 4194304
  172.2 10.3 %all-gather.7.cloned.1.call-done = bf16[8192,128]{1,0:T(8,128)(2,1)} async-done(((bf16[1024,128]{1,0:T(8,128)(2,1)}), bf16[8192,128]{1,0:T(8,128)(2,1)}) %all-gather.7.cloned.1.call-update) | async-done | bytes 2097168 | tf_op jit(solution)/shard_map/all_gather | solution.py:20
  182.6 3.9 %copy.49 = bf16[16,512,1,128]{1,3,2,0:T(8,128)(2,1)} copy(bf16[16,512,1,128]{3,1,0,2:T(8,128)(2,1)} %bitcast.98) | data formatting | bytes 4194304
  186.6 24.3 %while.15 = (s32[]{:T(128)}, f32[256,1,2]{0,2,1:T(2,128)S(1)}, f32[256,1,2]{0,2,1:T(2,128)S(1)}, f32[256,1,2,128]{0,3,2,1:T(8,128)S(1)}, s32[16]{0:T(128)S(1)}, ...) while((s32[]{:T(128)}, f32[256,1,2]{0,2,1:T(2,128)S(1)}, ...), condition=%wide.region_5.6_spmd.clone, body=%wide.region_0.5_spmd.clone.sunk | while | flops 103287040 | bytes 4563285 | solution.py:82
  187.8 4.0 %conditional.3 = ((f32[256,1,2]{0,2,1:T(2,128)S(1)}, f32[256,1,2]{0,2,1:T(2,128)S(1)}, f32[256,1,2,128]{0,3,2,1:T(8,128)S(1)})) conditional(s32[]{:T(128)} %convert_element_type.73, (f32[256,1,2]{0,2,1:T(2,128)S(1)}, f32[256,1,2]{0,2,1:T(2,128)S(1)}, f32[256,1,2,128]{0,3,2,1:T(8,128)S(1)}) %tuple.42, (s32[]{:T(128)}, s32[]{:T(128)}, s32[]{:T(128)}, ...), branch_computations={%region_1.1_spmd, %region_2.4_spmd} | conditional | flops 103287040 | bytes 4562002 | solution.py:78
  211.9 39.5 %reduce-scatter.4.cloned.1.call-done = bf16[128,1024]{1,0:T(8,128)(2,1)} async-done(((bf16[2048,1024]{1,0:T(8,128)(2,1)}), bf16[128,1024]{1,0:T(8,128)(2,1)}) %reduce-scatter.4.cloned.1.call-update) | async-done | bytes 262160
  251.4 1.8 reshape.281
  253.3 1.8 copy.59
  255.1 25.9 %all-to-all-start.1 = ((bf16[32,32,128]{2,1,0:T(8,128)(2,1)}), bf16[32,32,128]{2,1,0:T(8,128)(2,1)S(1)}, u32[]{:S(2)}, u32[]{:S(2)}) async-start(bf16[32,32,128]{2,1,0:T(8,128)(2,1)} %copy.59), calls=%async_computation.1 | async-start | bytes 524288 | tf_op jit(solution)/shard_map/all_to_all | solution.py:145
  281.1 32.9 %all-gather.9.cloned.1.call-done = bf16[256,2048]{0,1:T(8,128)(2,1)} async-done(((bf16[256,128]{0,1:T(8,128)(2,1)}), bf16[256,2048]{0,1:T(8,128)(2,1)}) %all-gather.9.cloned.1.call-update) | async-done | bytes 1048592 | tf_op jit(solution)/shard_map/all_gather | solution.py:93
  314.0 2.3 convolution_convert_fusion.1
  (129 shorter events, 22.5 us)
Async XLA Ops:
  7.2 96.6 %copy-start = (bf16[1,256,2048]{2,1,0:T(8,128)(2,1)S(1)}, bf16[1,256,2048]{2,1,0:T(8,128)(2,1)}, u32[]{:S(2)}) copy-start(bf16[1,256,2048]{2,1,0:T(8,128)(2,1)} %param.31) | copy-start | bytes 3145732
  7.2 91.6 %all-gather.11.cloned.1.call-start = ((), (), s32[]{:S(2)}) async-start(), calls=%async_computation.6 | async-start | bytes 4456448 | tf_op jit(solution)/shard_map/all_gather | solution.py:133
  16.5 32.0 %copy-start.3 = (bf16[256,128]{1,0:T(8,128)(2,1)S(1)}, bf16[256,128]{1,0:T(8,128)(2,1)}, u32[]{:S(2)}) copy-start(bf16[256,128]{1,0:T(8,128)(2,1)} %param.19) | copy-start | bytes 196612
  16.5 42.8 %copy-start.4 = (bf16[256,128]{1,0:T(8,128)(2,1)S(1)}, bf16[256,128]{1,0:T(8,128)(2,1)}, u32[]{:S(2)}) copy-start(bf16[256,128]{1,0:T(8,128)(2,1)} %param.20) | copy-start | bytes 196612
  16.5 82.3 %copy-start.9 = (bf16[1,2048,256]{2,1,0:T(8,128)(2,1)S(1)}, bf16[1,2048,256]{2,1,0:T(8,128)(2,1)}, u32[]{:S(2)}) copy-start(bf16[1,2048,256]{2,1,0:T(8,128)(2,1)} %param.29) | copy-start | bytes 3145732
  48.5 106.4 %all-gather.5.cloned.1.call-start = ((), (), s32[]{:S(2)}) async-start(), calls=%async_computation.3 | async-start | bytes 2359296 | tf_op jit(solution)/shard_map/all_gather | solution.py:20
  59.3 43.2 %copy-start.10 = (bf16[1,2048,256]{2,1,0:T(8,128)(2,1)S(1)}, bf16[1,2048,256]{2,1,0:T(8,128)(2,1)}, u32[]{:S(2)}) copy-start(bf16[1,2048,256]{2,1,0:T(8,128)(2,1)} %param.30) | copy-start | bytes 3145732
  59.3 123.3 %all-gather.7.cloned.1.call-start = ((), (), s32[]{:S(2)}) async-start(), calls=%async_computation.4 | async-start | bytes 2359296 | tf_op jit(solution)/shard_map/all_gather | solution.py:20
  70.5 180.9 %reduce-scatter.4.cloned.1.call-start = ((), (), s32[]{:S(2)}) async-start(), calls=%async_computation.7 | async-start | bytes 4456448
  98.8 3.6 %copy-start.8 = (bf16[32,32,2048]{2,1,0:T(8,128)(2,1)S(1)}, bf16[32,32,2048]{2,1,0:T(8,128)(2,1)}, u32[]{:S(2)}) copy-start(bf16[32,32,2048]{2,1,0:T(8,128)(2,1)} %all-gather.11.cloned.1.call-done) | copy-start | bytes 12582916
  153.3 0.8 copy-start.5
  153.3 160.7 %all-gather.9.cloned.1.call-start = ((), (), s32[]{:S(2)}) async-start(), calls=%async_computation.5 | async-start | bytes 1114112 | tf_op jit(solution)/shard_map/all_gather | solution.py:93
  186.5 24.4 %copy-start.7 = (f32[128]{0:T(128)S(1)}, f32[128]{0:T(128)}, u32[]{:S(2)}) copy-start(f32[128]{0:T(128)} %param.22) | copy-start | bytes 1540
  186.6 25.2 %copy-start.2 = (f32[256,8]{0,1:T(8,128)S(1)}, f32[256,8]{0,1:T(8,128)}, u32[]{:S(2)}) copy-start(f32[256,8]{0,1:T(8,128)} %param.27) | copy-start | bytes 24580
  186.6 25.2 %copy-start.6 = (f32[256,2]{0,1:T(2,128)S(1)}, f32[256,2]{0,1:T(2,128)}, u32[]{:S(2)}) copy-start(f32[256,2]{0,1:T(2,128)} %param.28) | copy-start | bytes 6148
  210.9 103.1 %copy-start.1 = (bf16[2048,128]{1,0:T(8,128)(2,1)S(1)}, bf16[2048,128]{1,0:T(8,128)(2,1)}, u32[]{:S(2)}) copy-start(bf16[2048,128]{1,0:T(8,128)(2,1)} %param.23) | copy-start | bytes 1572868
  255.1 61.3 %all-to-all-start.1 = ((bf16[32,32,128]{2,1,0:T(8,128)(2,1)}), bf16[32,32,128]{2,1,0:T(8,128)(2,1)S(1)}, u32[]{:S(2)}, u32[]{:S(2)}) async-start(bf16[32,32,128]{2,1,0:T(8,128)(2,1)} %copy.59), calls=%async_computation.1 | async-start | bytes 524288 | tf_op jit(solution)/shard_map/all_to_all | solution.py:145
Sparse Core Ops, SparseCore 0:
  48.6 50.1 all-gather.10
  100.9 37.4 all-gather.4
  140.5 42.0 all-gather.6
  185.3 66.1 reduce-scatter.3
  254.0 59.9 all-gather.8
where the time goes:
time: 328 us; the launch traced here: 325 us
  waiting for transfers between devices  111 us (34%)
  local copies, waits for them, and re-layouts  94.1 us (29%)
  blocking collectives  46.8 us (14%)
  starting transfers between devices  26.3 us (8%)
  between operations  14.8 us (5%)
  loops' own time  12.6 us (4%)
  matrix products  12.1 us (4%)
  other arithmetic  7.48 us (2%)
    unnamed x30, local copies, waits for them, and re-layouts  64.6 us
    unnamed x6, waiting for transfers between devices  39.6 us
    all_gather x1, waiting for transfers between devices, token_mixer(): lax.all_gather(head_out, 'tp', axis=1, tiled=True)  32.9 us
    all_gather x1, waiting for transfers between devices, expert_block(): experts_arrived = lax.all_gather(arrived, 'tp', axis=2, tiled=True)  28.3 us
    all_to_all x1, starting transfers between devices, expert_block(): lax.all_to_all(answered, EP, split_axis=0, concat_axis=0, tiled=True)  25.9 us
    all_to_all x1, blocking collectives, expert_block(): lax.all_to_all(own_columns, EP, split_axis=0, concat_axis=0, tiled=True)  24.9 us
    all_gather x2, blocking collectives, whole_of(): nearer = lax.all_gather(array, axes[-1], axis=dim, tiled=True)  21.8 us
    another operation x1, loops' own time, token_mixer(): lax.scan(update, state_now, jnp.arange(blocks, dtype=jnp.int32))  10.6 us
  transfers between devices with their start and end apart: 6, of which 4 were waited for; matrix products, arithmetic and copies ran while one was open for 29% of the time, Pallas kernels for 0%

commit v1 on v0

v1 whole, which is shorter than its diff:
```python
import jax
import jax.numpy as jnp
from jax import lax
from jax.experimental import pallas as pl
from jax.experimental.pallas import tpu as pltpu
from jax.sharding import Mesh
from jax.sharding import PartitionSpec as P

EPSILON = 1e-05
LOWEST = -1e30
GROUP_SIZE = 4
LANES = 128
CHUNKS = 4
F32 = jnp.float32
BF16 = jnp.bfloat16


def remote(src, dst, send_sem, recv_sem, **where):
    return pltpu.make_async_remote_copy(
        src_ref=src,
        dst_ref=dst,
        send_sem=send_sem,
        recv_sem=recv_sem,
        device_id=where,
        device_id_type=pl.DeviceIdType.MESH,
    )


def loop(first, last, body):
    def step(i, carry):
        body(i)
        return carry

    lax.fori_loop(first, last, step, 0)


def kernel(
    sizes,
    q_ref,
    k_ref,
    v_ref,
    scale_ref,
    hgain_ref,
    ow_hbm,
    rin_ref,
    rgain_ref,
    ids_ref,
    gl_ref,
    il_ref,
    gw_hbm,
    uw_hbm,
    dw_hbm,
    mix_ref,
    rout_ref,
    gw,
    uw,
    dw,
    ow,
    w_sem,
    pos0,
    pos1,
    rw0,
    rw1,
    disp,
    xs,
    parts,
    mate,
    rb_up,
    rb_dn,
    sb_up,
    sb_dn,
    ans,
    ret,
    a_send,
    a_recv,
    up_send,
    up_recv,
    dn_send,
    dn_recv,
    m_send,
    m_recv,
    pm_send,
    pm_recv,
    ru_send,
    ru_recv,
    rd_send,
    rd_recv,
    b_send,
    b_recv,
    qb,
    qs,
    kb,
    vb,
    acc,
    stat,
    o_out,
    o_in,
    stat_in,
    heads,
    q_send,
    q_recv,
    k_send,
    k_recv,
    v_send,
    v_recv,
    o_send,
    o_recv,
    s_send,
    s_recv,
    h_send,
    h_recv,
    hm_send,
    hm_recv,
):
    nz, nx, ny = sizes
    nep = nz * nx
    half_ring = ny // 2
    z, x, y, c = (lax.axis_index(name) for name in ("z", "x", "y", "c"))
    other = 1 - c
    e = z * nx + x
    t = y * 2 + c
    rows = rin_ref.shape[0]
    width = rin_ref.shape[1]
    total = xs.shape[2]
    cap = total // nep
    chunk = total // CHUNKS
    half = chunk // 2
    per_chunk = nep // CHUNKS
    y_next = lax.rem(y + 1, ny)
    y_prev = lax.rem(y + ny - 1, ny)

    def y_at(shift):
        return lax.rem(y + shift + ny, ny)

    def ep_at(shift):
        peer = lax.rem(e + shift, nep)
        return peer, peer // nx, lax.rem(peer, nx)

    barrier = pltpu.get_barrier_semaphore()

    def greet(r):
        _, pz, px = ep_at(r)
        pl.semaphore_signal(
            barrier, inc=1, device_id={"z": pz, "x": px}, device_id_type=pl.DeviceIdType.MESH
        )

    loop(1, nep, greet)

    def greet_y(r):
        pl.semaphore_signal(
            barrier, inc=1, device_id={"y": lax.rem(y + r, ny)}, device_id_type=pl.DeviceIdType.MESH
        )

    loop(1, ny, greet_y)
    pl.semaphore_signal(
        barrier, inc=1, device_id={"c": other}, device_id_type=pl.DeviceIdType.MESH
    )

    weight_copies = [
        pltpu.make_async_copy(src, dst, w_sem.at[i])
        for i, (src, dst) in enumerate(
            ((gw_hbm, gw), (uw_hbm, uw), (dw_hbm, dw), (ow_hbm, ow))
        )
    ]
    for copy in weight_copies:
        copy.start()

    own_cols = pl.ds(pl.multiple_of(t * LANES, LANES), LANES)
    source = rin_ref[...].astype(F32)
    inv = lax.rsqrt(jnp.sum(source * source, axis=-1, keepdims=True) * (1.0 / width) + EPSILON)
    normed = (rin_ref[:, own_cols].astype(F32) * inv * rgain_ref[:, own_cols]).astype(BF16)
    id0 = ids_ref[:, 0:1]
    id1 = ids_ref[:, 1:2]
    lane = lax.broadcasted_iota(jnp.int32, (rows, LANES), 1)
    pick0 = jnp.where(id0 == lane, 1.0, 0.0)
    pick1 = jnp.where(id1 == lane, 1.0, 0.0)
    below = jnp.where(
        lax.broadcasted_iota(jnp.int32, (rows, rows), 0)
        > lax.broadcasted_iota(jnp.int32, (rows, rows), 1),
        1.0,
        0.0,
    ).astype(BF16)
    before0 = jnp.dot(below, pick0.astype(BF16), preferred_element_type=F32)
    before1 = jnp.dot(below, pick1.astype(BF16), preferred_element_type=F32) + jnp.sum(
        pick0, axis=0, keepdims=True
    )
    pos0[...] = id0.astype(F32) * cap + jnp.sum(pick0 * before0, axis=1, keepdims=True)
    pos1[...] = id1.astype(F32) * cap + jnp.sum(pick1 * before1, axis=1, keepdims=True)

    def one_hot(pos):
        slots = lax.broadcasted_iota(jnp.int32, (rows, total), 1).astype(F32)
        return jnp.where(pos[...] == slots, 1.0, 0.0).astype(BF16)

    disp[...] = lax.dot_general(
        one_hot(pos0) + one_hot(pos1),
        normed,
        (((0,), (0,)), ((), ())),
        preferred_element_type=F32,
    ).astype(BF16)
    logits = gl_ref[...]
    group_exp = jnp.exp(logits - jnp.max(logits, axis=-1, keepdims=True))
    group_prob = group_exp / jnp.sum(group_exp, axis=-1, keepdims=True)
    groups = lax.broadcasted_iota(jnp.int32, logits.shape, 1)
    inner = il_ref[...]
    inner_exp = jnp.exp(inner - jnp.max(inner, axis=-1, keepdims=True))
    inner_prob = inner_exp / jnp.sum(inner_exp, axis=-1, keepdims=True)
    for number, weight in ((0, rw0), (1, rw1)):
        chosen = ids_ref[:, number : number + 1] // GROUP_SIZE
        picked = jnp.sum(jnp.where(chosen == groups, group_prob, 0.0), axis=1, keepdims=True)
        weight[...] = picked * inner_prob[:, number : number + 1]

    pl.semaphore_wait(barrier, nep - 1 + ny - 1 + 1)

    def slot_rows(index):
        return pl.ds(pl.multiple_of(index * cap, cap), cap)

    def dispatch(r):
        peer, pz, px = ep_at(r)
        return remote(
            disp.at[slot_rows(peer)],
            xs.at[y, c, slot_rows(e)],
            a_send.at[r],
            a_recv.at[r],
            z=pz,
            x=px,
        )

    loop(1, nep, lambda r: dispatch(r).start())
    xs[y, c, slot_rows(e), :] = disp[slot_rows(e), :]

    def query_copy(r):
        return remote(
            q_ref, qb.at[x], q_send.at[r], q_recv.at[r], x=lax.rem(x + r, nx)
        )

    for r in range(1, nx):
        query_copy(r).start()

    def key_copies(r):
        return (
            remote(k_ref, kb.at[z], k_send.at[r], k_recv.at[r], z=lax.rem(z + r, nz)),
            remote(v_ref, vb.at[z], v_send.at[r], v_recv.at[r], z=lax.rem(z + r, nz)),
        )

    for r in range(1, nz):

        @pl.when(z + r < nz)
        def _(r=r):
            for copy in key_copies(r):
                copy.start()

    maps = 2 * rows
    qk = LANES // 2
    keep_low = lax.broadcasted_iota(jnp.int32, (rows, LANES), 1) < qk

    def stack_query(value, index):
        scaled = value.astype(F32) * (qk ** (-0.5))
        qs[index, 0:rows, :] = jnp.where(keep_low, scaled, 0.0).astype(BF16)
        qs[index, rows:maps, :] = jnp.where(keep_low, 0.0, scaled).astype(BF16)

    def attend(key_block, value_block, masked):
        def one(index):
            scores = lax.dot_general(
                key_block[...],
                qs[index],
                (((1,), (1,)), ((), ())),
                preferred_element_type=F32,
            )
            if masked:
                key_pos = x * rows + lax.broadcasted_iota(jnp.int32, scores.shape, 0)
                column = lax.broadcasted_iota(jnp.int32, scores.shape, 1)
                query_pos = index * rows + jnp.where(column >= rows, column - rows, column)
                visible = query_pos >= key_pos
                scores = jnp.where(visible, scores, LOWEST)
                new_max = jnp.max(scores, axis=0, keepdims=True)
                terms = jnp.where(visible, jnp.exp(scores - new_max), 0.0)
                stat[index, 1:2, :] = jnp.sum(terms, axis=0, keepdims=True)
            else:
                old_max = stat[index, 0:1, :]
                new_max = jnp.maximum(old_max, jnp.max(scores, axis=0, keepdims=True))
                terms = jnp.exp(scores - new_max)
                factor = jnp.exp(old_max - new_max)
                stat[index, 1:2, :] = stat[index, 1:2, :] * factor + jnp.sum(
                    terms, axis=0, keepdims=True
                )
            stat[index, 0:1, :] = new_max
            weighted = lax.dot_general(
                value_block[...],
                terms.astype(BF16),
                (((0,), (0,)), ((), ())),
                preferred_element_type=F32,
            )
            if masked:
                acc[index] = weighted
            else:
                acc[index] = acc[index] * factor + weighted

        loop(0, nx, one)

    stack_query(q_ref[...], x)
    for r in range(1, nx):
        query_copy(r).wait_recv()
        from_x = lax.rem(x + nx - r, nx)
        stack_query(qb[from_x], from_x)
    stat[...] = jnp.zeros_like(stat)
    attend(k_ref, v_ref, True)

    def attend_far(r):
        if r < nz:

            @pl.when(z >= r)
            def _():
                for copy in key_copies(r):
                    copy.wait_recv()
                from_z = jnp.maximum(z - r, 0)
                attend(kb.at[from_z], vb.at[from_z], False)

    def wait_dispatch(r):
        from_e = lax.rem(e + nep - r, nep)
        remote(
            disp.at[slot_rows(0)],
            xs.at[y, c, slot_rows(from_e)],
            a_send.at[r],
            a_recv.at[r],
            z=z,
            x=x,
        ).wait_recv()

    loop(1, nep, wait_dispatch)

    def chunk_rows(k):
        return pl.ds(pl.multiple_of(k * chunk, chunk), chunk)

    def upper_rows(k):
        return pl.ds(pl.multiple_of(k * chunk, half), half)

    def lower_rows(k):
        return pl.ds(pl.multiple_of(k * chunk + half, half), half)

    def up_copy(s, k):
        where = upper_rows(k) if s == half_ring - 1 else chunk_rows(k)
        block = xs.at[y_at(-s), c, where]
        return remote(block, block, up_send.at[k, s], up_recv.at[k, s], y=y_next)

    def dn_copy(s, k):
        where = lower_rows(k) if s == half_ring - 1 else chunk_rows(k)
        block = xs.at[y_at(s), c, where]
        return remote(block, block, dn_send.at[k, s], dn_recv.at[k, s], y=y_prev)

    def up_arrival(s, k):
        where = upper_rows(k) if s == half_ring - 1 else chunk_rows(k)
        block = xs.at[y_at(-s - 1), c, where]
        return remote(block, block, up_send.at[k, s], up_recv.at[k, s], y=y_next)

    def dn_arrival(s, k):
        where = lower_rows(k) if s == half_ring - 1 else chunk_rows(k)
        block = xs.at[y_at(s + 1), c, where]
        return remote(block, block, dn_send.at[k, s], dn_recv.at[k, s], y=y_prev)

    def mate_blocks(k, core):
        blocks = [xs.at[y, core, chunk_rows(k)]]
        for s in range(half_ring):
            last = s == half_ring - 1
            blocks.append(
                xs.at[y_at(-s - 1), core, upper_rows(k) if last else chunk_rows(k)]
            )
            blocks.append(
                xs.at[y_at(s + 1), core, lower_rows(k) if last else chunk_rows(k)]
            )
        return blocks

    def mate_copy(number, k):
        block = mate_blocks(k, c)[number]
        return remote(block, block, m_send.at[k, number], m_recv.at[k, number], c=other)

    def mate_arrival(number, k):
        block = mate_blocks(k, other)[number]
        return remote(block, block, m_send.at[k, number], m_recv.at[k, number], c=other)

    def first_sends(k):
        up_copy(0, k).start()
        dn_copy(0, k).start()
        mate_copy(0, k).start()

    loop(0, CHUNKS, first_sends)
    attend_far(1)
    attend_far(2)
    for s in range(half_ring):

        def pass_on(k, s=s):
            up_arrival(s, k).wait_recv()
            if s + 1 < half_ring:
                up_copy(s + 1, k).start()
            mate_copy(2 * s + 1, k).start()
            dn_arrival(s, k).wait_recv()
            if s + 1 < half_ring:
                dn_copy(s + 1, k).start()
            mate_copy(2 * s + 2, k).start()

        loop(0, CHUNKS, pass_on)
        if s < half_ring - 1:
            attend_far(2 * s + 3)
            attend_far(2 * s + 4)
    for r in range(2 * half_ring + 1, nz):
        attend_far(r)

    def result_copies(r):
        to_x = lax.rem(x + r, nx)
        return (
            remote(o_out.at[to_x], o_in.at[x], o_send.at[r], o_recv.at[r], x=to_x),
            remote(stat.at[to_x], stat_in.at[x], s_send.at[r], s_recv.at[r], x=to_x),
        )

    def result_arrivals(r):
        from_x = lax.rem(x + nx - r, nx)
        return (
            remote(o_out.at[0], o_in.at[from_x], o_send.at[r], o_recv.at[r], x=x),
            remote(stat.at[0], stat_in.at[from_x], s_send.at[r], s_recv.at[r], x=x),
        )

    o_out[...] = acc[...].astype(BF16)
    for r in range(1, nx):
        for copy in result_copies(r):
            copy.start()
    o_in[x] = o_out[x]
    stat_in[x] = stat[x]

    for copy in weight_copies[:3]:
        copy.wait()

    def expert(k):
        for number in range(2 * half_ring + 1):
            mate_arrival(number, k).wait_recv()
        gate = jnp.zeros((chunk, gw.shape[1]), F32)
        up = jnp.zeros((chunk, gw.shape[1]), F32)
        for block in range(ny):
            both = jnp.concatenate(
                [xs[block, 0, chunk_rows(k), :], xs[block, 1, chunk_rows(k), :]], axis=1
            )
            depth = slice(block * 2 * LANES, (block + 1) * 2 * LANES)
            gate += jnp.dot(both, gw[depth, :], preferred_element_type=F32)
            up += jnp.dot(both, uw[depth, :], preferred_element_type=F32)
        hidden = (gate / (1.0 + jnp.exp(-gate)) * up).astype(BF16)
        for block in range(ny):
            columns = slice(block * 2 * LANES, (block + 1) * 2 * LANES)
            value = jnp.dot(hidden, dw[:, columns], preferred_element_type=F32).astype(BF16)
            parts[k, 0, block] = value[:, :LANES]
            parts[k, 1, block] = value[:, LANES:]
        part_copy(k).start()

    def part_copy(k):
        return remote(parts.at[k, other], mate.at[k], pm_send.at[k], pm_recv.at[k], c=other)

    full = slice(0, chunk)
    top = slice(0, half)
    bottom = slice(half, chunk)

    def chip_sum(k, target, where):
        return parts[k, c, target, where, :].astype(F32) + mate[k, target, where, :].astype(F32)

    def sum_up(k, d):
        where = top if d == half_ring else full
        return remote(
            sb_up.at[k, d - 1, where], rb_up.at[k, d - 1, where],
            ru_send.at[k, d - 1], ru_recv.at[k, d - 1], y=y_next,
        )

    def sum_dn(k, d):
        where = bottom if d == half_ring else full
        return remote(
            sb_dn.at[k, d - 1, where], rb_dn.at[k, d - 1, where],
            rd_send.at[k, d - 1], rd_recv.at[k, d - 1], y=y_prev,
        )

    def sum_step(k, d):
        if d == half_ring:
            sb_up[k, d - 1, top] = chip_sum(k, y_at(d), top).astype(BF16)
            sum_up(k, d).start()
            sb_dn[k, d - 1, bottom] = chip_sum(k, y_at(-d), bottom).astype(BF16)
            sum_dn(k, d).start()
            return
        sum_up(k, d + 1).wait_recv()
        if d + 1 == half_ring:
            sb_up[k, d - 1, top] = (
                chip_sum(k, y_at(d), top) + rb_up[k, d, top].astype(F32)
            ).astype(BF16)
            sb_up[k, d - 1, bottom] = chip_sum(k, y_at(d), bottom).astype(BF16)
        else:
            sb_up[k, d - 1] = (
                chip_sum(k, y_at(d), full) + rb_up[k, d].astype(F32)
            ).astype(BF16)
        sum_up(k, d).start()
        sum_dn(k, d + 1).wait_recv()
        if d + 1 == half_ring:
            sb_dn[k, d - 1, bottom] = (
                chip_sum(k, y_at(-d), bottom) + rb_dn[k, d, bottom].astype(F32)
            ).astype(BF16)
            sb_dn[k, d - 1, top] = chip_sum(k, y_at(-d), top).astype(BF16)
        else:
            sb_dn[k, d - 1] = (
                chip_sum(k, y_at(-d), full) + rb_dn[k, d].astype(F32)
            ).astype(BF16)
        sum_dn(k, d).start()

    def answer(k):
        sum_up(k, 1).wait_recv()
        sum_dn(k, 1).wait_recv()
        if half_ring > 1:
            ans[chunk_rows(k), :] = (
                chip_sum(k, y, full) + rb_up[k, 0].astype(F32) + rb_dn[k, 0].astype(F32)
            ).astype(BF16)
        else:
            ans[upper_rows(k), :] = (
                chip_sum(k, y, top) + rb_up[k, 0, top].astype(F32)
            ).astype(BF16)
            ans[lower_rows(k), :] = (
                chip_sum(k, y, bottom) + rb_dn[k, 0, bottom].astype(F32)
            ).astype(BF16)

        def reply(j):
            target = k * per_chunk + j

            @pl.when(target != e)
            def _():
                back_copy(target).start()

        loop(0, per_chunk, reply)

    def back_copy(target):
        return remote(
            ans.at[slot_rows(target)],
            ret.at[slot_rows(e)],
            b_send.at[target],
            b_recv.at[e],
            z=target // nx,
            x=lax.rem(target, nx),
        )

    def first_sum(k):
        part_copy(k).wait_recv()
        sum_step(k, half_ring)

    loop(0, 1, expert)

    def expert_and_sum(k):
        expert(k)
        first_sum(k - 1)

    loop(1, CHUNKS, expert_and_sum)
    loop(CHUNKS - 1, CHUNKS, first_sum)

    def head_copy(r):
        return remote(
            heads.at[y, c], heads.at[y, c], h_send.at[r], h_recv.at[r], y=lax.rem(y + r, ny)
        )

    def head_mate(r):
        block = heads.at[lax.rem(y + ny - r, ny), c]
        return remote(block, block, hm_send.at[r], hm_recv.at[r], c=other)

    def merge():
        for r in range(1, nx):
            for copy in result_arrivals(r):
                copy.wait_recv()
        top_max = stat_in[0, 0:1, :]
        for j in range(1, nx):
            top_max = jnp.maximum(top_max, stat_in[j, 0:1, :])
        denominator = jnp.zeros_like(top_max)
        weighted = jnp.zeros(o_in.shape[1:], F32)
        for j in range(nx):
            factor = jnp.exp(stat_in[j, 0:1, :] - top_max)
            denominator += factor * stat_in[j, 1:2, :]
            weighted += factor * o_in[j].astype(F32)
        mapped = weighted / denominator
        difference = mapped[:, :rows] - scale_ref[0:1, 0:1] * mapped[:, rows:]
        mean = jnp.sum(difference * difference, axis=0, keepdims=True) * (1.0 / LANES)
        head = difference * lax.rsqrt(mean + EPSILON) * hgain_ref[...]
        heads[y, c] = head.T.astype(BF16)
        for r in range(1, ny):
            head_copy(r).start()
        head_mate(0).start()

    merge()

    if half_ring > 1:
        loop(0, CHUNKS, lambda k: sum_step(k, half_ring - 1))

    for r in range(1, ny):
        arrived = heads.at[lax.rem(y + ny - r, ny), c]
        remote(arrived, arrived, h_send.at[r], h_recv.at[r], y=y_next).wait_recv()
        head_mate(r).start()

    for d in range(half_ring - 2, 0, -1):
        loop(0, CHUNKS, lambda k, d=d: sum_step(k, d))
    loop(0, CHUNKS, answer)
    ret[slot_rows(e), :] = ans[slot_rows(e), :]

    weight_copies[3].wait()
    for r in range(ny):
        arrived = heads.at[lax.rem(y + ny - r, ny), other]
        remote(arrived, arrived, hm_send.at[r], hm_recv.at[r], c=other).wait_recv()
    mixed = jnp.zeros((rows, LANES), F32)
    for block in range(ny):
        both = jnp.concatenate([heads[block, 0], heads[block, 1]], axis=1)
        mixed += jnp.dot(
            both, ow[block * 2 * LANES : (block + 1) * 2 * LANES, :], preferred_element_type=F32
        )
    mix_ref[...] = mixed.astype(BF16)

    def wait_back(r):
        from_e = lax.rem(e + nep - r, nep)
        remote(
            ans.at[slot_rows(0)],
            ret.at[slot_rows(from_e)],
            b_send.at[from_e],
            b_recv.at[from_e],
            z=z,
            x=x,
        ).wait_recv()

    loop(1, nep, wait_back)
    first = jnp.dot(one_hot(pos0), ret[...], preferred_element_type=F32)
    second = jnp.dot(one_hot(pos1), ret[...], preferred_element_type=F32)
    rout_ref[...] = (rw0[...] * first + rw1[...] * second).astype(BF16)

    def drain(r):
        dispatch(r).wait_send()
        peer, _, _ = ep_at(r)
        back_copy(peer).wait_send()

    loop(1, nep, drain)

    def drain_chunk(k):
        for s in range(half_ring):
            up_copy(s, k).wait_send()
            dn_copy(s, k).wait_send()
            sum_up(k, s + 1).wait_send()
            sum_dn(k, s + 1).wait_send()
        for number in range(2 * half_ring + 1):
            mate_copy(number, k).wait_send()
        part_copy(k).wait_send()

    loop(0, CHUNKS, drain_chunk)
    for r in range(1, nx):
        query_copy(r).wait_send()
        for copy in result_copies(r):
            copy.wait_send()
    for r in range(1, nz):

        @pl.when(z + r < nz)
        def _(r=r):
            for copy in key_copies(r):
                copy.wait_send()

    for r in range(1, ny):
        head_copy(r).wait_send()
    for r in range(ny):
        head_mate(r).wait_send()


def local(
    sizes,
    queries,
    key_rows,
    values,
    second_scale,
    head_gain,
    out_weight,
    routed_in,
    routed_gain,
    expert_ids,
    group_logits,
    inner_logits,
    gate_weight,
    up_weight,
    down_weight,
):
    nz, nx, ny = sizes
    nep = nz * nx
    rows = routed_in.shape[0]
    width = routed_in.shape[1]
    hidden = gate_weight.shape[2]
    cap = 2 * expert_ids.shape[1] * rows // nep
    total = nep * cap
    chunk = total // CHUNKS
    half_ring = ny // 2
    mates = 2 * half_ring + 1
    dma = pltpu.SemaphoreType.DMA
    vmem = pltpu.VMEM
    scratch = [
        vmem((width, hidden), BF16),
        vmem((width, hidden), BF16),
        vmem((hidden, width), BF16),
        vmem(out_weight.shape, BF16),
        dma((4,)),
        vmem((rows, 1), F32),
        vmem((rows, 1), F32),
        vmem((rows, 1), F32),
        vmem((rows, 1), F32),
        vmem((total, LANES), BF16),
        vmem((ny, 2, total, LANES), BF16),
        vmem((CHUNKS, 2, ny, chunk, LANES), BF16),
        vmem((CHUNKS, ny, chunk, LANES), BF16),
        vmem((CHUNKS, half_ring, chunk, LANES), BF16),
        vmem((CHUNKS, half_ring, chunk, LANES), BF16),
        vmem((CHUNKS, half_ring, chunk, LANES), BF16),
        vmem((CHUNKS, half_ring, chunk, LANES), BF16),
        vmem((total, LANES), BF16),
        vmem((total, LANES), BF16),
        dma((nep,)),
        dma((nep,)),
        dma((CHUNKS, half_ring)),
        dma((CHUNKS, half_ring)),
        dma((CHUNKS, half_ring)),
        dma((CHUNKS, half_ring)),
        dma((CHUNKS, mates)),
        dma((CHUNKS, mates)),
        dma((CHUNKS,)),
        dma((CHUNKS,)),
        dma((CHUNKS, half_ring)),
        dma((CHUNKS, half_ring)),
        dma((CHUNKS, half_ring)),
        dma((CHUNKS, half_ring)),
        dma((nep,)),
        dma((nep,)),
        vmem((nx, rows, LANES), BF16),
        vmem((nx, 2 * rows, LANES), BF16),
        vmem((nz, rows, LANES), BF16),
        vmem((nz, rows, LANES), BF16),
        vmem((nx, LANES, 2 * rows), F32),
        vmem((nx, 8, 2 * rows), F32),
        vmem((nx, LANES, 2 * rows), BF16),
        vmem((nx, LANES, 2 * rows), BF16),
        vmem((nx, 8, 2 * rows), F32),
        vmem((ny, 2, rows, LANES), BF16),
        dma((nx,)),
        dma((nx,)),
        dma((nz,)),
        dma((nz,)),
        dma((nz,)),
        dma((nz,)),
        dma((nx,)),
        dma((nx,)),
        dma((nx,)),
        dma((nx,)),
        dma((ny,)),
        dma((ny,)),
        dma((ny,)),
        dma((ny,)),
    ]
    whole = pl.BlockSpec(memory_space=pltpu.VMEM)
    far = pl.BlockSpec(memory_space=pl.ANY)
    return pl.pallas_call(
        lambda *refs: kernel(sizes, *refs),
        out_shape=(
            jax.ShapeDtypeStruct((rows, LANES), BF16),
            jax.ShapeDtypeStruct((rows, LANES), BF16),
        ),
        in_specs=[whole, whole, whole, whole, whole, far, whole, whole, whole, whole, whole, far, far, far],
        out_specs=(whole, whole),
        scratch_shapes=scratch,
        compiler_params=pltpu.CompilerParams(
            collective_id=0, has_side_effects=True, vmem_limit_bytes=60 * 1024 * 1024
        ),
    )(
        queries,
        key_rows,
        values,
        second_scale.reshape(1, 1),
        head_gain.reshape(-1, 1),
        out_weight,
        routed_in,
        routed_gain.reshape(1, -1),
        expert_ids,
        group_logits,
        inner_logits,
        gate_weight[0],
        up_weight[0],
        down_weight[0],
    )


def build(mesh, sizes):
    nz, nx, ny = sizes
    finer = Mesh(mesh.devices.reshape(nz, nx, ny, 2), ("z", "x", "y", "c"))
    ep, tp = ("z", "x"), ("y", "c")
    placed = (
        P(ep, tp),
        P(ep, tp),
        P(ep, tp),
        P(tp),
        P(),
        P(None, tp),
        P(ep, None),
        P(),
        P(ep, None),
        P(ep, None),
        P(ep, None),
        P(ep, None, tp),
        P(ep, None, tp),
        P(ep, tp, None),
    )
    return jax.shard_map(
        lambda *args: local(sizes, *args),
        mesh=finer,
        in_specs=placed,
        out_specs=(P(ep, tp), P(ep, tp)),
        check_vma=False,
    )


def solution(mesh):
    return build(mesh, (8, 4, mesh.shape["tp"] // 2))
```

time: 328 us -> 114 us (0.35)
  waiting for transfers between devices: 111 us -> 0 us
  Pallas kernels: 0 us -> 106 us
  local copies, waits for them, and re-layouts: 94.1 us -> 5.9 us
  blocking collectives: 46.8 us -> 0 us
  starting transfers between devices: 26.3 us -> 0 us
  between operations: 14.8 us -> 1.31 us
  loops' own time: 12.6 us -> 0 us
  matrix products: 12.1 us -> 0 us
  other arithmetic: 7.48 us -> 0 us
    pallas_call x0 -> x1, Pallas kernels: none -> 106 us  [local(): pl.pallas_call(lambda *refs: kernel(sizes, *refs), out_shape=(jax.ShapeDt...]
    all_gather x4 -> x0, waiting for transfers between devices: 71.5 us -> none  [the longest x1 32.9 us: token_mixer(): lax.all_gather(head_out, 'tp', axis=1, tiled=True)]
    unnamed x30 -> x15, local copies, waits for them, and re-layouts: 64.6 us -> 5.16 us
    unnamed x6 -> x0, waiting for transfers between devices: 39.6 us -> none
    all_to_all x1 -> x0, starting transfers between devices: 25.9 us -> none  [expert_block(): lax.all_to_all(answered, EP, split_axis=0, concat_axis=0, tiled=True)]
    all_to_all x1 -> x0, blocking collectives: 24.9 us -> none  [expert_block(): lax.all_to_all(own_columns, EP, split_axis=0, concat_axis=0, tiled=True)]
    all_gather x2 -> x0, blocking collectives: 21.8 us -> none  [whole_of(): nearer = lax.all_gather(array, axes[-1], axis=dim, tiled=True)]
    another operation x17 -> x0, loops' own time: 12.6 us -> none  [the longest x1 10.6 us: token_mixer(): lax.scan(update, state_now, jnp.arange(blocks, dtype=jnp.int32))]
  transfers between devices with their start and end apart: 6 -> 0, of which waited for: 4 -> 0; matrix products, arithmetic and copies ran while one was open for 29% -> 0% of each run, Pallas kernels for 0% -> 0%
where the time goes in v1:
time: 114 us; the launch traced here: 113 us
  Pallas kernels  106 us (93%)
  local copies, waits for them, and re-layouts  5.9 us (5%)
  between operations  1.31 us (1%)
    pallas_call x1, Pallas kernels, local(): pl.pallas_call(lambda *refs: kernel(sizes, *refs), out_shape=(jax.ShapeDt...  106 us
    unnamed x15, local copies, waits for them, and re-layouts  5.16 us

profile of v1, /device:TPU:1, one launch (start us, length us, event | category | flops | bytes accessed | tf_op | source)
XLA Modules:
  0.0 112.8 jit_solution(5266833002233308692)
XLA Ops:
  1.3 0.0 copy-start.4
  1.3 0.6 copy-done.4
  1.9 0.0 copy-start.2
  1.9 0.7 copy.16.refs_4_
  2.7 0.0 copy-done.2
  2.7 0.0 copy-start.1
  2.7 0.8 copy.17.refs_8_
  3.5 0.0 copy-done.1
  3.5 0.0 copy-start.3
  3.5 0.8 copy.18.refs_9_
  4.3 0.0 copy-done.3
  4.3 0.8 copy.19.refs_10_
  5.0 105.6 %shard_map.149 = (bf16[256,128]{1,0:T(8,128)(2,1)}, bf16[256,128]{1,0:T(8,128)(2,1)}) custom-call(bf16[256,128]{1,0:T(8,128)(2,1)} %refs_0_.1, bf16[256,128]{1,0:T(8,128)(2,1)} %refs_1_.1, bf16[256,128]{1,0:T(8,128)(2,1)} %refs_2_.1, f32[1,1]{1,0:T(1,128)} %bitcast.6.refs_3_, f32[128,1]{1,0:T(8,128)} %copy.16.refs_4_, bf16[2048,128]{1,0:T(8,128)(2,1)} %refs_5_.1, ...), custom_call_target="tpu_custom_call" | custom-call | tf_op jit(solution)/shard_map/pallas_call | solution.py:753
  110.7 0.0 copy-start
  110.7 1.5 %copy.23 = bf16[256,128]{1,0:T(8,128)(2,1)} copy(bf16[256,128]{1,0:T(8,128)(2,1)} %get-tuple-element.4) | data formatting | bytes 131072
  112.2 0.0 copy-done
  112.2 0.6 copy.24
Async XLA Ops:
  1.3 0.7 copy-start.4
  1.9 0.7 copy-start.2
  2.7 0.8 copy-start.1
  3.5 0.8 copy-start.3
  110.7 1.5 %copy-start = (bf16[256,128]{1,0:T(8,128)(2,1)S(1)}, bf16[256,128]{1,0:T(8,128)(2,1)}, u32[]{:S(2)}) copy-start(bf16[256,128]{1,0:T(8,128)(2,1)} %get-tuple-element.5) | copy-start | bytes 196612

commit v2 on v1

--- a/solution.py
+++ b/solution.py
@@ -36,13 +36,13 @@
 
 def kernel(
     sizes,
-    q_ref,
-    k_ref,
-    v_ref,
+    q_hbm,
+    k_hbm,
+    v_hbm,
     scale_ref,
     hgain_ref,
     ow_hbm,
-    rin_ref,
+    rin_hbm,
     rgain_ref,
     ids_ref,
     gl_ref,
@@ -56,11 +56,11 @@
     uw,
     dw,
     ow,
+    rin,
     w_sem,
-    pos0,
-    pos1,
-    rw0,
-    rw1,
+    i_sem,
+    pos,
+    weight,
     disp,
     xs,
     parts,
@@ -107,8 +107,10 @@
     o_recv,
     s_send,
     s_recv,
-    h_send,
-    h_recv,
+    hu_send,
+    hu_recv,
+    hd_send,
+    hd_recv,
     hm_send,
     hm_recv,
 ):
@@ -119,8 +121,8 @@
     other = 1 - c
     e = z * nx + x
     t = y * 2 + c
-    rows = rin_ref.shape[0]
-    width = rin_ref.shape[1]
+    rows = rin.shape[0]
+    width = rin.shape[1]
     total = xs.shape[2]
     cap = total // nep
     chunk = total // CHUNKS
@@ -132,19 +134,30 @@
     def y_at(shift):
         return lax.rem(y + shift + ny, ny)
 
-    def ep_at(shift):
-        peer = lax.rem(e + shift, nep)
-        return peer, peer // nx, lax.rem(peer, nx)
+    group = z // (nz // CHUNKS)
+
+    def nearby(j):
+        return lax.rem(group + j + j // 2 - 2 * (j // 3), CHUNKS)
+
+    def each_other(first, count, body):
+        def one(i):
+            @pl.when(first + i != e)
+            def _():
+                body(first + i)
+
+        loop(0, count, one)
 
     barrier = pltpu.get_barrier_semaphore()
 
-    def greet(r):
-        _, pz, px = ep_at(r)
+    def greet(peer):
         pl.semaphore_signal(
-            barrier, inc=1, device_id={"z": pz, "x": px}, device_id_type=pl.DeviceIdType.MESH
-        )
-
-    loop(1, nep, greet)
+            barrier,
+            inc=1,
+            device_id={"z": peer // nx, "x": lax.rem(peer, nx)},
+            device_id_type=pl.DeviceIdType.MESH,
+        )
+
+    each_other(0, nep, greet)
 
     def greet_y(r):
         pl.semaphore_signal(
@@ -156,98 +169,122 @@
         barrier, inc=1, device_id={"c": other}, device_id_type=pl.DeviceIdType.MESH
     )
 
+    input_copies = [
+        pltpu.make_async_copy(src, dst, i_sem.at[i])
+        for i, (src, dst) in enumerate(
+            ((rin_hbm, rin), (q_hbm, qb.at[x]), (k_hbm, kb.at[z]), (v_hbm, vb.at[z]))
+        )
+    ]
     weight_copies = [
         pltpu.make_async_copy(src, dst, w_sem.at[i])
         for i, (src, dst) in enumerate(
             ((gw_hbm, gw), (uw_hbm, uw), (dw_hbm, dw), (ow_hbm, ow))
         )
     ]
-    for copy in weight_copies:
+    for copy in input_copies + weight_copies:
         copy.start()
 
-    own_cols = pl.ds(pl.multiple_of(t * LANES, LANES), LANES)
-    source = rin_ref[...].astype(F32)
-    inv = lax.rsqrt(jnp.sum(source * source, axis=-1, keepdims=True) * (1.0 / width) + EPSILON)
-    normed = (rin_ref[:, own_cols].astype(F32) * inv * rgain_ref[:, own_cols]).astype(BF16)
-    id0 = ids_ref[:, 0:1]
-    id1 = ids_ref[:, 1:2]
-    lane = lax.broadcasted_iota(jnp.int32, (rows, LANES), 1)
-    pick0 = jnp.where(id0 == lane, 1.0, 0.0)
-    pick1 = jnp.where(id1 == lane, 1.0, 0.0)
-    below = jnp.where(
+    ids = ids_ref[...]
+    shape = (nep, rows)
+    expert_row = lax.broadcasted_iota(jnp.int32, shape, 0)
+    picks = [jnp.where(ids[i : i + 1, :] == expert_row, 1.0, 0.0) for i in range(2)]
+    earlier = jnp.where(
         lax.broadcasted_iota(jnp.int32, (rows, rows), 0)
-        > lax.broadcasted_iota(jnp.int32, (rows, rows), 1),
+        < lax.broadcasted_iota(jnp.int32, (rows, rows), 1),
         1.0,
         0.0,
     ).astype(BF16)
-    before0 = jnp.dot(below, pick0.astype(BF16), preferred_element_type=F32)
-    before1 = jnp.dot(below, pick1.astype(BF16), preferred_element_type=F32) + jnp.sum(
-        pick0, axis=0, keepdims=True
-    )
-    pos0[...] = id0.astype(F32) * cap + jnp.sum(pick0 * before0, axis=1, keepdims=True)
-    pos1[...] = id1.astype(F32) * cap + jnp.sum(pick1 * before1, axis=1, keepdims=True)
-
-    def one_hot(pos):
-        slots = lax.broadcasted_iota(jnp.int32, (rows, total), 1).astype(F32)
-        return jnp.where(pos[...] == slots, 1.0, 0.0).astype(BF16)
-
-    disp[...] = lax.dot_general(
-        one_hot(pos0) + one_hot(pos1),
-        normed,
-        (((0,), (0,)), ((), ())),
-        preferred_element_type=F32,
+    before = [jnp.dot(pick.astype(BF16), earlier, preferred_element_type=F32) for pick in picks]
+    before[1] += jnp.sum(picks[0], axis=1, keepdims=True)
+    logits = gl_ref[...]
+    group_exp = jnp.exp(logits - jnp.max(logits, axis=0, keepdims=True))
+    group_prob = group_exp / jnp.sum(group_exp, axis=0, keepdims=True)
+    group_row = lax.broadcasted_iota(jnp.int32, logits.shape, 0)
+    inner = il_ref[...]
+    inner_exp = jnp.exp(inner - jnp.max(inner, axis=0, keepdims=True))
+    inner_prob = inner_exp / jnp.sum(inner_exp, axis=0, keepdims=True)
+    for i in range(2):
+        pos[i : i + 1, :] = ids[i : i + 1, :].astype(F32) * cap + jnp.sum(
+            picks[i] * before[i], axis=0, keepdims=True
+        )
+        chosen = ids[i : i + 1, :] // GROUP_SIZE == group_row
+        picked = jnp.sum(jnp.where(chosen, group_prob, 0.0), axis=0, keepdims=True)
+        weight[i : i + 1, :] = picked * inner_prob[i : i + 1, :]
+
+    def one_hot(i):
+        slots = lax.broadcasted_iota(jnp.int32, (total, rows), 0).astype(F32)
+        return jnp.where(pos[i : i + 1, :] == slots, 1.0, 0.0).astype(BF16)
+
+    own_cols = pl.ds(pl.multiple_of(t * LANES, LANES), LANES)
+    input_copies[0].wait()
+    source = rin[...].astype(F32)
+    inv = lax.rsqrt(jnp.sum(source * source, axis=-1, keepdims=True) * (1.0 / width) + EPSILON)
+    normed = (rin[:, own_cols].astype(F32) * inv * rgain_ref[:, own_cols]).astype(BF16)
+    disp[...] = jnp.dot(
+        one_hot(0) + one_hot(1), normed, preferred_element_type=F32
     ).astype(BF16)
-    logits = gl_ref[...]
-    group_exp = jnp.exp(logits - jnp.max(logits, axis=-1, keepdims=True))
-    group_prob = group_exp / jnp.sum(group_exp, axis=-1, keepdims=True)
-    groups = lax.broadcasted_iota(jnp.int32, logits.shape, 1)
-    inner = il_ref[...]
-    inner_exp = jnp.exp(inner - jnp.max(inner, axis=-1, keepdims=True))
-    inner_prob = inner_exp / jnp.sum(inner_exp, axis=-1, keepdims=True)
-    for number, weight in ((0, rw0), (1, rw1)):
-        chosen = ids_ref[:, number : number + 1] // GROUP_SIZE
-        picked = jnp.sum(jnp.where(chosen == groups, group_prob, 0.0), axis=1, keepdims=True)
-        weight[...] = picked * inner_prob[:, number : number + 1]
+    for copy in input_copies[1:]:
+        copy.wait()
 
     pl.semaphore_wait(barrier, nep - 1 + ny - 1 + 1)
 
     def slot_rows(index):
         return pl.ds(pl.multiple_of(index * cap, cap), cap)
 
-    def dispatch(r):
-        peer, pz, px = ep_at(r)
+    def dispatch(peer):
         return remote(
             disp.at[slot_rows(peer)],
             xs.at[y, c, slot_rows(e)],
-            a_send.at[r],
-            a_recv.at[r],
-            z=pz,
-            x=px,
-        )
-
-    loop(1, nep, lambda r: dispatch(r).start())
+            a_send.at[peer],
+            a_recv.at[e],
+            z=peer // nx,
+            x=lax.rem(peer, nx),
+        )
+
+    loop(
+        0,
+        CHUNKS,
+        lambda j: each_other(
+            nearby(j) * per_chunk, per_chunk, lambda peer: dispatch(peer).start()
+        ),
+    )
     xs[y, c, slot_rows(e), :] = disp[slot_rows(e), :]
 
     def query_copy(r):
         return remote(
-            q_ref, qb.at[x], q_send.at[r], q_recv.at[r], x=lax.rem(x + r, nx)
-        )
+            qb.at[x], qb.at[x], q_send.at[r], q_recv.at[r], x=lax.rem(x + r, nx)
+        )
+
+    reach = nz // 2
+
+    def key_copies(block, r, to_z):
+        return (
+            remote(kb.at[block], kb.at[block], k_send.at[r], k_recv.at[r], z=to_z),
+            remote(vb.at[block], vb.at[block], v_send.at[r], v_recv.at[r], z=to_z),
+        )
+
+    def chain_copies(r):
+        return key_copies(jnp.maximum(z - r + 1, 0), r, jnp.minimum(z + 1, nz - 1))
+
+    def far_copies(r):
+        return key_copies(z, r, lax.rem(z + r, nz))
+
+    def chain_send(r):
+        @pl.when((z + 1 < nz) & (z - r + 1 >= 0))
+        def _():
+            for copy in chain_copies(r):
+                copy.start()
+
+    chain_send(1)
+    for r in range(reach + 1, nz):
+
+        @pl.when(z + r < nz)
+        def _(r=r):
+            for copy in far_copies(r):
+                copy.start()
 
     for r in range(1, nx):
         query_copy(r).start()
-
-    def key_copies(r):
-        return (
-            remote(k_ref, kb.at[z], k_send.at[r], k_recv.at[r], z=lax.rem(z + r, nz)),
-            remote(v_ref, vb.at[z], v_send.at[r], v_recv.at[r], z=lax.rem(z + r, nz)),
-        )
-
-    for r in range(1, nz):
-
-        @pl.when(z + r < nz)
-        def _(r=r):
-            for copy in key_copies(r):
-                copy.start()
 
     maps = 2 * rows
     qk = LANES // 2
@@ -297,36 +334,34 @@
 
         loop(0, nx, one)
 
-    stack_query(q_ref[...], x)
-    for r in range(1, nx):
-        query_copy(r).wait_recv()
-        from_x = lax.rem(x + nx - r, nx)
-        stack_query(qb[from_x], from_x)
-    stat[...] = jnp.zeros_like(stat)
-    attend(k_ref, v_ref, True)
+    def own_attention():
+        stack_query(qb[x], x)
+        for r in range(1, nx):
+            query_copy(r).wait_recv()
+            from_x = lax.rem(x + nx - r, nx)
+            stack_query(qb[from_x], from_x)
+        stat[...] = jnp.zeros_like(stat)
+        attend(kb.at[z], vb.at[z], True)
 
     def attend_far(r):
-        if r < nz:
-
-            @pl.when(z >= r)
-            def _():
-                for copy in key_copies(r):
-                    copy.wait_recv()
-                from_z = jnp.maximum(z - r, 0)
-                attend(kb.at[from_z], vb.at[from_z], False)
-
-    def wait_dispatch(r):
-        from_e = lax.rem(e + nep - r, nep)
+        @pl.when(z >= r)
+        def _():
+            from_z = jnp.maximum(z - r, 0)
+            for copy in key_copies(from_z, r, z):
+                copy.wait_recv()
+            if r < reach:
+                chain_send(r + 1)
+            attend(kb.at[from_z], vb.at[from_z], False)
+
+    def wait_dispatch(peer):
         remote(
             disp.at[slot_rows(0)],
-            xs.at[y, c, slot_rows(from_e)],
-            a_send.at[r],
-            a_recv.at[r],
+            xs.at[y, c, slot_rows(peer)],
+            a_send.at[peer],
+            a_recv.at[peer],
             z=z,
             x=x,
         ).wait_recv()
-
-    loop(1, nep, wait_dispatch)
 
     def chunk_rows(k):
         return pl.ds(pl.multiple_of(k * chunk, chunk), chunk)
@@ -377,17 +412,16 @@
         block = mate_blocks(k, other)[number]
         return remote(block, block, m_send.at[k, number], m_recv.at[k, number], c=other)
 
-    def first_sends(k):
+    def first_sends(j):
+        k = nearby(j)
+        each_other(k * per_chunk, per_chunk, wait_dispatch)
         up_copy(0, k).start()
         dn_copy(0, k).start()
         mate_copy(0, k).start()
 
-    loop(0, CHUNKS, first_sends)
-    attend_far(1)
-    attend_far(2)
-    for s in range(half_ring):
-
-        def pass_on(k, s=s):
+    def pass_on(s):
+        def one(j):
+            k = nearby(j)
             up_arrival(s, k).wait_recv()
             if s + 1 < half_ring:
                 up_copy(s + 1, k).start()
@@ -397,12 +431,20 @@
                 dn_copy(s + 1, k).start()
             mate_copy(2 * s + 2, k).start()
 
-        loop(0, CHUNKS, pass_on)
-        if s < half_ring - 1:
-            attend_far(2 * s + 3)
-            attend_far(2 * s + 4)
-    for r in range(2 * half_ring + 1, nz):
-        attend_far(r)
+        loop(0, CHUNKS, one)
+
+    loop(0, CHUNKS, first_sends)
+    own_attention()
+    attend_far(1)
+    pass_on(0)
+    attend_far(2)
+    attend_far(3)
+    pass_on(1)
+    attend_far(4)
+    attend_far(5)
+    pass_on(2)
+    attend_far(6)
+    attend_far(7)
 
     def result_copies(r):
         to_x = lax.rem(x + r, nx)
@@ -425,10 +467,12 @@
     o_in[x] = o_out[x]
     stat_in[x] = stat[x]
 
+    pass_on(3)
     for copy in weight_copies[:3]:
         copy.wait()
 
-    def expert(k):
+    def expert(j):
+        k = nearby(j)
         for number in range(2 * half_ring + 1):
             mate_arrival(number, k).wait_recv()
         gate = jnp.zeros((chunk, gw.shape[1]), F32)
@@ -517,14 +561,7 @@
                 chip_sum(k, y, bottom) + rb_dn[k, 0, bottom].astype(F32)
             ).astype(BF16)
 
-        def reply(j):
-            target = k * per_chunk + j
-
-            @pl.when(target != e)
-            def _():
-                back_copy(target).start()
-
-        loop(0, per_chunk, reply)
+        each_other(k * per_chunk, per_chunk, lambda target: back_copy(target).start())
 
     def back_copy(target):
         return remote(
@@ -536,27 +573,54 @@
             x=lax.rem(target, nx),
         )
 
-    def first_sum(k):
+    def first_sum(j):
+        k = nearby(j)
         part_copy(k).wait_recv()
         sum_step(k, half_ring)
 
     loop(0, 1, expert)
 
-    def expert_and_sum(k):
-        expert(k)
-        first_sum(k - 1)
+    def expert_and_sum(j):
+        expert(j)
+        first_sum(j - 1)
 
     loop(1, CHUNKS, expert_and_sum)
     loop(CHUNKS - 1, CHUNKS, first_sum)
 
-    def head_copy(r):
-        return remote(
-            heads.at[y, c], heads.at[y, c], h_send.at[r], h_recv.at[r], y=lax.rem(y + r, ny)
-        )
-
-    def head_mate(r):
-        block = heads.at[lax.rem(y + ny - r, ny), c]
-        return remote(block, block, hm_send.at[r], hm_recv.at[r], c=other)
+    top_rows = pl.ds(0, rows // 2)
+    low_rows = pl.ds(rows // 2, rows // 2)
+    all_rows = pl.ds(0, rows)
+
+    def head_up(s, hop):
+        where = top_rows if s == half_ring - 1 else all_rows
+        block = heads.at[y_at(-s - hop), c, where]
+        return remote(block, block, hu_send.at[s], hu_recv.at[s], y=y_next)
+
+    def head_dn(s, hop):
+        where = low_rows if s == half_ring - 1 else all_rows
+        block = heads.at[y_at(s + hop), c, where]
+        return remote(block, block, hd_send.at[s], hd_recv.at[s], y=y_prev)
+
+    def head_mate(number, core):
+        s = (number - 1) // 2
+        last = number > 0 and s == half_ring - 1
+        if number == 0:
+            block = heads.at[y, core]
+        elif number % 2 == 1:
+            block = heads.at[y_at(-s - 1), core, top_rows if last else all_rows]
+        else:
+            block = heads.at[y_at(s + 1), core, low_rows if last else all_rows]
+        return remote(block, block, hm_send.at[number], hm_recv.at[number], c=other)
+
+    def head_pass(s):
+        head_up(s, 1).wait_recv()
+        if s + 1 < half_ring:
+            head_up(s + 1, 0).start()
+        head_mate(2 * s + 1, c).start()
+        head_dn(s, 1).wait_recv()
+        if s + 1 < half_ring:
+            head_dn(s + 1, 0).start()
+        head_mate(2 * s + 2, c).start()
 
     def merge():
         for r in range(1, nx):
@@ -574,31 +638,30 @@
         mapped = weighted / denominator
         difference = mapped[:, :rows] - scale_ref[0:1, 0:1] * mapped[:, rows:]
         mean = jnp.sum(difference * difference, axis=0, keepdims=True) * (1.0 / LANES)
-        head = difference * lax.rsqrt(mean + EPSILON) * hgain_ref[...]
-        heads[y, c] = head.T.astype(BF16)
-        for r in range(1, ny):
-            head_copy(r).start()
-        head_mate(0).start()
+        head = difference * lax.rsqrt(mean + EPSILON)
+        heads[y, c] = (head.T * hgain_ref[...]).astype(BF16)
+        head_up(0, 0).start()
+        head_dn(0, 0).start()
+        head_mate(0, c).start()
 
     merge()
 
-    if half_ring > 1:
-        loop(0, CHUNKS, lambda k: sum_step(k, half_ring - 1))
-
-    for r in range(1, ny):
-        arrived = heads.at[lax.rem(y + ny - r, ny), c]
-        remote(arrived, arrived, h_send.at[r], h_recv.at[r], y=y_next).wait_recv()
-        head_mate(r).start()
-
-    for d in range(half_ring - 2, 0, -1):
-        loop(0, CHUNKS, lambda k, d=d: sum_step(k, d))
-    loop(0, CHUNKS, answer)
+    def sums(d):
+        loop(0, CHUNKS, lambda j: sum_step(nearby(j), d))
+
+    sums(3)
+    head_pass(0)
+    sums(2)
+    head_pass(1)
+    sums(1)
+    head_pass(2)
+    loop(0, CHUNKS, lambda j: answer(nearby(j)))
     ret[slot_rows(e), :] = ans[slot_rows(e), :]
+    head_pass(3)
 
     weight_copies[3].wait()
-    for r in range(ny):
-        arrived = heads.at[lax.rem(y + ny - r, ny), other]
-        remote(arrived, arrived, hm_send.at[r], hm_recv.at[r], c=other).wait_recv()
+    for number in range(2 * half_ring + 1):
+        head_mate(number, other).wait_recv()
     mixed = jnp.zeros((rows, LANES), F32)
     for block in range(ny):
         both = jnp.concatenate([heads[block, 0], heads[block, 1]], axis=1)
@@ -607,28 +670,29 @@
         )
     mix_ref[...] = mixed.astype(BF16)
 
-    def wait_back(r):
-        from_e = lax.rem(e + nep - r, nep)
+    def wait_back(peer):
         remote(
             ans.at[slot_rows(0)],
-            ret.at[slot_rows(from_e)],
-            b_send.at[from_e],
-            b_recv.at[from_e],
+            ret.at[slot_rows(peer)],
+            b_send.at[peer],
+            b_recv.at[peer],
             z=z,
             x=x,
         ).wait_recv()
 
-    loop(1, nep, wait_back)
-    first = jnp.dot(one_hot(pos0), ret[...], preferred_element_type=F32)
-    second = jnp.dot(one_hot(pos1), ret[...], preferred_element_type=F32)
-    rout_ref[...] = (rw0[...] * first + rw1[...] * second).astype(BF16)
-
-    def drain(r):
-        dispatch(r).wait_send()
-        peer, _, _ = ep_at(r)
+    each_other(0, nep, wait_back)
+    routed = jnp.zeros((LANES, rows), F32)
+    for i in range(2):
+        routed += weight[i : i + 1, :] * lax.dot_general(
+            ret[...], one_hot(i), (((0,), (0,)), ((), ())), preferred_element_type=F32
+        )
+    rout_ref[...] = routed.T.astype(BF16)
+
+    def drain(peer):
+        dispatch(peer).wait_send()
         back_copy(peer).wait_send()
 
-    loop(1, nep, drain)
+    each_other(0, nep, drain)
 
     def drain_chunk(k):
         for s in range(half_ring):
@@ -645,17 +709,25 @@
         query_copy(r).wait_send()
         for copy in result_copies(r):
             copy.wait_send()
-    for r in range(1, nz):
+    for r in range(1, reach + 1):
+
+        @pl.when((z + 1 < nz) & (z - r + 1 >= 0))
+        def _(r=r):
+            for copy in chain_copies(r):
+                copy.wait_send()
+
+    for r in range(reach + 1, nz):
 
         @pl.when(z + r < nz)
         def _(r=r):
-            for copy in key_copies(r):
+            for copy in far_copies(r):
                 copy.wait_send()
 
-    for r in range(1, ny):
-        head_copy(r).wait_send()
-    for r in range(ny):
-        head_mate(r).wait_send()
+    for s in range(half_ring):
+        head_up(s, 0).wait_send()
+        head_dn(s, 0).wait_send()
+    for number in range(2 * half_ring + 1):
+        head_mate(number, c).wait_send()
 
 
 def local(
@@ -692,11 +764,11 @@
         vmem((width, hidden), BF16),
         vmem((hidden, width), BF16),
         vmem(out_weight.shape, BF16),
+        vmem((rows, width), BF16),
         dma((4,)),
-        vmem((rows, 1), F32),
-        vmem((rows, 1), F32),
-        vmem((rows, 1), F32),
-        vmem((rows, 1), F32),
+        dma((4,)),
+        vmem((8, rows), F32),
+        vmem((8, rows), F32),
         vmem((total, LANES), BF16),
         vmem((ny, 2, total, LANES), BF16),
         vmem((CHUNKS, 2, ny, chunk, LANES), BF16),
@@ -743,10 +815,12 @@
         dma((nx,)),
         dma((nx,)),
         dma((nx,)),
-        dma((ny,)),
-        dma((ny,)),
-        dma((ny,)),
-        dma((ny,)),
+        dma((half_ring,)),
+        dma((half_ring,)),
+        dma((half_ring,)),
+        dma((half_ring,)),
+        dma((mates,)),
+        dma((mates,)),
     ]
     whole = pl.BlockSpec(memory_space=pltpu.VMEM)
     far = pl.BlockSpec(memory_space=pl.ANY)
@@ -756,7 +830,7 @@
             jax.ShapeDtypeStruct((rows, LANES), BF16),
             jax.ShapeDtypeStruct((rows, LANES), BF16),
         ),
-        in_specs=[whole, whole, whole, whole, whole, far, whole, whole, whole, whole, whole, far, far, far],
+        in_specs=[far] * 3 + [whole] * 2 + [far] * 2 + [whole] * 4 + [far] * 3,
         out_specs=(whole, whole),
         scratch_shapes=scratch,
         compiler_params=pltpu.CompilerParams(
@@ -767,13 +841,13 @@
         key_rows,
         values,
         second_scale.reshape(1, 1),
-        head_gain.reshape(-1, 1),
+        head_gain.reshape(1, -1),
         out_weight,
         routed_in,
         routed_gain.reshape(1, -1),
-        expert_ids,
-        group_logits,
-        inner_logits,
+        expert_ids.T,
+        group_logits.T,
+        inner_logits.T,
         gate_weight[0],
         up_weight[0],
         down_weight[0],

time: 114 us -> 99.9 us (0.88)
  Pallas kernels: 106 us -> 95.8 us
  local copies, waits for them, and re-layouts: 5.9 us -> 2.14 us
    pallas_call x1, Pallas kernels: 106 us -> 95.8 us  [local(): pl.pallas_call(lambda *refs: kernel(sizes, *refs), out_shape=(jax.ShapeDt...]
    unnamed x15 -> x4, local copies, waits for them, and re-layouts: 5.16 us -> 2.14 us
where the time goes in v2:
time: 99.9 us; the launch traced here: 99.3 us
  Pallas kernels  95.8 us (96%)
  local copies, waits for them, and re-layouts  2.14 us (2%)
  between operations  1.3 us (1%)
    pallas_call x1, Pallas kernels, local(): pl.pallas_call(lambda *refs: kernel(sizes, *refs), out_shape=(jax.ShapeDt...  95.8 us
    unnamed x4, local copies, waits for them, and re-layouts  2.14 us

profile of v2, /device:TPU:1, one launch (start us, length us, event | category | flops | bytes accessed | tf_op | source)
XLA Modules:
  0.0 99.3 jit_solution(18078124276248439862)
XLA Ops:
  1.3 95.8 %shard_map.149 = (bf16[256,128]{1,0:T(8,128)(2,1)}, bf16[256,128]{1,0:T(8,128)(2,1)}) custom-call(bf16[256,128]{1,0:T(8,128)(2,1)} %refs_0_.1, bf16[256,128]{1,0:T(8,128)(2,1)} %refs_1_.1, bf16[256,128]{1,0:T(8,128)(2,1)} %refs_2_.1, f32[1,1]{1,0:T(1,128)} %bitcast.9.refs_3_, f32[1,128]{1,0:T(1,128)} %bitcast.17, bf16[2048,128]{1,0:T(8,128)(2,1)} %refs_5_.1, ...), custom_call_target="tpu_custom_call" | custom-call | tf_op jit(solution)/shard_map/pallas_call | solution.py:827
  97.1 0.0 copy-start
  97.1 1.5 %copy.19 = bf16[256,128]{1,0:T(8,128)(2,1)} copy(bf16[256,128]{1,0:T(8,128)(2,1)} %get-tuple-element.4) | data formatting | bytes 131072
  98.6 0.0 copy-done
  98.6 0.6 copy.20
Async XLA Ops:
  97.1 1.5 %copy-start = (bf16[256,128]{1,0:T(8,128)(2,1)S(1)}, bf16[256,128]{1,0:T(8,128)(2,1)}, u32[]{:S(2)}) copy-start(bf16[256,128]{1,0:T(8,128)(2,1)} %get-tuple-element.5) | copy-start | bytes 196612

commit v3 on v2

--- a/solution.py
+++ b/solution.py
@@ -39,14 +39,14 @@
     q_hbm,
     k_hbm,
     v_hbm,
-    scale_ref,
-    hgain_ref,
+    scale_hbm,
+    hgain_hbm,
     ow_hbm,
     rin_hbm,
-    rgain_ref,
-    ids_ref,
-    gl_ref,
-    il_ref,
+    rgain_hbm,
+    ids_hbm,
+    gl_hbm,
+    il_hbm,
     gw_hbm,
     uw_hbm,
     dw_hbm,
@@ -57,6 +57,12 @@
     dw,
     ow,
     rin,
+    scale_ref,
+    hgain_ref,
+    rgain_ref,
+    ids_ref,
+    gl_ref,
+    il_ref,
     w_sem,
     i_sem,
     pos,
@@ -137,7 +143,7 @@
     group = z // (nz // CHUNKS)
 
     def nearby(j):
-        return lax.rem(group + j + j // 2 - 2 * (j // 3), CHUNKS)
+        return lax.rem(group + (0, 1, 3, 2)[j], CHUNKS)
 
     def each_other(first, count, body):
         def one(i):
@@ -172,7 +178,18 @@
     input_copies = [
         pltpu.make_async_copy(src, dst, i_sem.at[i])
         for i, (src, dst) in enumerate(
-            ((rin_hbm, rin), (q_hbm, qb.at[x]), (k_hbm, kb.at[z]), (v_hbm, vb.at[z]))
+            (
+                (ids_hbm, ids_ref),
+                (gl_hbm, gl_ref),
+                (il_hbm, il_ref),
+                (rgain_hbm, rgain_ref),
+                (rin_hbm, rin),
+                (q_hbm, qb.at[x]),
+                (k_hbm, kb.at[z]),
+                (v_hbm, vb.at[z]),
+                (scale_hbm, scale_ref),
+                (hgain_hbm, hgain_ref),
+            )
         )
     ]
     weight_copies = [
@@ -184,6 +201,8 @@
     for copy in input_copies + weight_copies:
         copy.start()
 
+    for copy in input_copies[:4]:
+        copy.wait()
     ids = ids_ref[...]
     shape = (nep, rows)
     expert_row = lax.broadcasted_iota(jnp.int32, shape, 0)
@@ -216,14 +235,14 @@
         return jnp.where(pos[i : i + 1, :] == slots, 1.0, 0.0).astype(BF16)
 
     own_cols = pl.ds(pl.multiple_of(t * LANES, LANES), LANES)
-    input_copies[0].wait()
+    input_copies[4].wait()
     source = rin[...].astype(F32)
     inv = lax.rsqrt(jnp.sum(source * source, axis=-1, keepdims=True) * (1.0 / width) + EPSILON)
     normed = (rin[:, own_cols].astype(F32) * inv * rgain_ref[:, own_cols]).astype(BF16)
     disp[...] = jnp.dot(
         one_hot(0) + one_hot(1), normed, preferred_element_type=F32
     ).astype(BF16)
-    for copy in input_copies[1:]:
+    for copy in input_copies[5:]:
         copy.wait()
 
     pl.semaphore_wait(barrier, nep - 1 + ny - 1 + 1)
@@ -241,13 +260,8 @@
             x=lax.rem(peer, nx),
         )
 
-    loop(
-        0,
-        CHUNKS,
-        lambda j: each_other(
-            nearby(j) * per_chunk, per_chunk, lambda peer: dispatch(peer).start()
-        ),
-    )
+    for j in range(CHUNKS):
+        each_other(nearby(j) * per_chunk, per_chunk, lambda peer: dispatch(peer).start())
     xs[y, c, slot_rows(e), :] = disp[slot_rows(e), :]
 
     def query_copy(r):
@@ -275,16 +289,17 @@
             for copy in chain_copies(r):
                 copy.start()
 
-    chain_send(1)
-    for r in range(reach + 1, nz):
-
-        @pl.when(z + r < nz)
-        def _(r=r):
-            for copy in far_copies(r):
-                copy.start()
-
-    for r in range(1, nx):
-        query_copy(r).start()
+    def send_queries_and_keys():
+        chain_send(1)
+        for r in range(reach + 1, nz):
+
+            @pl.when(z + r < nz)
+            def _(r=r):
+                for copy in far_copies(r):
+                    copy.start()
+
+        for r in range(1, nx):
+            query_copy(r).start()
 
     maps = 2 * rows
     qk = LANES // 2
@@ -343,14 +358,21 @@
         stat[...] = jnp.zeros_like(stat)
         attend(kb.at[z], vb.at[z], True)
 
+    def chain_step(r):
+        @pl.when(z >= r)
+        def _():
+            for copy in key_copies(jnp.maximum(z - r, 0), r, z):
+                copy.wait_recv()
+            if r < reach:
+                chain_send(r + 1)
+
     def attend_far(r):
         @pl.when(z >= r)
         def _():
             from_z = jnp.maximum(z - r, 0)
-            for copy in key_copies(from_z, r, z):
-                copy.wait_recv()
-            if r < reach:
-                chain_send(r + 1)
+            if r > reach:
+                for copy in key_copies(from_z, r, z):
+                    copy.wait_recv()
             attend(kb.at[from_z], vb.at[from_z], False)
 
     def wait_dispatch(peer):
@@ -412,39 +434,21 @@
         block = mate_blocks(k, other)[number]
         return remote(block, block, m_send.at[k, number], m_recv.at[k, number], c=other)
 
-    def first_sends(j):
-        k = nearby(j)
+    def first_sends(k):
         each_other(k * per_chunk, per_chunk, wait_dispatch)
         up_copy(0, k).start()
         dn_copy(0, k).start()
         mate_copy(0, k).start()
 
-    def pass_on(s):
-        def one(j):
-            k = nearby(j)
-            up_arrival(s, k).wait_recv()
-            if s + 1 < half_ring:
-                up_copy(s + 1, k).start()
-            mate_copy(2 * s + 1, k).start()
-            dn_arrival(s, k).wait_recv()
-            if s + 1 < half_ring:
-                dn_copy(s + 1, k).start()
-            mate_copy(2 * s + 2, k).start()
-
-        loop(0, CHUNKS, one)
-
-    loop(0, CHUNKS, first_sends)
-    own_attention()
-    attend_far(1)
-    pass_on(0)
-    attend_far(2)
-    attend_far(3)
-    pass_on(1)
-    attend_far(4)
-    attend_far(5)
-    pass_on(2)
-    attend_far(6)
-    attend_far(7)
+    def pass_on(s, k):
+        up_arrival(s, k).wait_recv()
+        if s + 1 < half_ring:
+            up_copy(s + 1, k).start()
+        mate_copy(2 * s + 1, k).start()
+        dn_arrival(s, k).wait_recv()
+        if s + 1 < half_ring:
+            dn_copy(s + 1, k).start()
+        mate_copy(2 * s + 2, k).start()
 
     def result_copies(r):
         to_x = lax.rem(x + r, nx)
@@ -460,19 +464,15 @@
             remote(stat.at[0], stat_in.at[from_x], s_send.at[r], s_recv.at[r], x=x),
         )
 
-    o_out[...] = acc[...].astype(BF16)
-    for r in range(1, nx):
-        for copy in result_copies(r):
-            copy.start()
-    o_in[x] = o_out[x]
-    stat_in[x] = stat[x]
-
-    pass_on(3)
-    for copy in weight_copies[:3]:
-        copy.wait()
-
-    def expert(j):
-        k = nearby(j)
+    def send_results():
+        o_out[...] = acc[...].astype(BF16)
+        for r in range(1, nx):
+            for copy in result_copies(r):
+                copy.start()
+        o_in[x] = o_out[x]
+        stat_in[x] = stat[x]
+
+    def expert(k):
         for number in range(2 * half_ring + 1):
             mate_arrival(number, k).wait_recv()
         gate = jnp.zeros((chunk, gw.shape[1]), F32)
@@ -573,19 +573,9 @@
             x=lax.rem(target, nx),
         )
 
-    def first_sum(j):
-        k = nearby(j)
+    def first_sum(k):
         part_copy(k).wait_recv()
         sum_step(k, half_ring)
-
-    loop(0, 1, expert)
-
-    def expert_and_sum(j):
-        expert(j)
-        first_sum(j - 1)
-
-    loop(1, CHUNKS, expert_and_sum)
-    loop(CHUNKS - 1, CHUNKS, first_sum)
 
     top_rows = pl.ds(0, rows // 2)
     low_rows = pl.ds(rows // 2, rows // 2)
@@ -644,20 +634,35 @@
         head_dn(0, 0).start()
         head_mate(0, c).start()
 
-    merge()
-
-    def sums(d):
-        loop(0, CHUNKS, lambda j: sum_step(nearby(j), d))
-
-    sums(3)
-    head_pass(0)
-    sums(2)
-    head_pass(1)
-    sums(1)
-    head_pass(2)
-    loop(0, CHUNKS, lambda j: answer(nearby(j)))
+    stages = [first_sends]
+    stages += [lambda k, s=s: pass_on(s, k) for s in range(half_ring)]
+    stages += [expert, first_sum]
+    stages += [lambda k, d=d: sum_step(k, d) for d in range(half_ring - 1, 0, -1)]
+    stages += [answer]
+    beside = {
+        0: [send_queries_and_keys],
+        2: [lambda: chain_step(1), own_attention],
+        3: [lambda: chain_step(2), lambda: attend_far(1)],
+        4: [lambda: chain_step(3), lambda: attend_far(2)],
+        5: [lambda: chain_step(4), lambda: attend_far(3)],
+        6: [lambda: attend_far(4), lambda: attend_far(5)],
+        7: [lambda: attend_far(6), lambda: attend_far(7), send_results],
+        9: [merge],
+        10: [lambda: head_pass(0)],
+        11: [lambda: head_pass(1)],
+        12: [lambda: head_pass(2)],
+        13: [lambda: head_pass(3)],
+    }
+    for wave in range(len(stages) + CHUNKS - 1):
+        for j in range(CHUNKS):
+            if 0 <= wave - j < len(stages):
+                if wave - j == half_ring + 1 and j == 0:
+                    for copy in weight_copies[:3]:
+                        copy.wait()
+                stages[wave - j](nearby(j))
+        for work in beside.get(wave, []):
+            work()
     ret[slot_rows(e), :] = ans[slot_rows(e), :]
-    head_pass(3)
 
     weight_copies[3].wait()
     for number in range(2 * half_ring + 1):
@@ -765,8 +770,14 @@
         vmem((hidden, width), BF16),
         vmem(out_weight.shape, BF16),
         vmem((rows, width), BF16),
+        vmem((1, 1), F32),
+        vmem((1, LANES), F32),
+        vmem((1, width), F32),
+        vmem((2, rows), jnp.int32),
+        vmem((group_logits.shape[1], rows), F32),
+        vmem((2, rows), F32),
         dma((4,)),
-        dma((4,)),
+        dma((10,)),
         vmem((8, rows), F32),
         vmem((8, rows), F32),
         vmem((total, LANES), BF16),
@@ -830,7 +841,7 @@
             jax.ShapeDtypeStruct((rows, LANES), BF16),
             jax.ShapeDtypeStruct((rows, LANES), BF16),
         ),
-        in_specs=[far] * 3 + [whole] * 2 + [far] * 2 + [whole] * 4 + [far] * 3,
+        in_specs=[far] * 14,
         out_specs=(whole, whole),
         scratch_shapes=scratch,
         compiler_params=pltpu.CompilerParams(

time: 99.9 us -> 95.1 us (0.952)
  the two profiles are of different devices: /device:TPU:1 before, /device:TPU:8 now
where the time goes in v3:
time: 95.1 us; the launch traced here: 94.9 us
  Pallas kernels  91.5 us (96%)
  local copies, waits for them, and re-layouts  2.14 us (2%)
  between operations  1.3 us (1%)
    pallas_call x1, Pallas kernels, local(): pl.pallas_call(lambda *refs: kernel(sizes, *refs), out_shape=(jax.ShapeDt...  91.5 us
    unnamed x4, local copies, waits for them, and re-layouts  2.14 us

profile of v3, /device:TPU:8, one launch (start us, length us, event | category | flops | bytes accessed | tf_op | source)
XLA Modules:
  0.0 94.9 jit_solution(12340455704805625749)
XLA Ops:
  1.3 91.5 %shard_map.149 = (bf16[256,128]{1,0:T(8,128)(2,1)}, bf16[256,128]{1,0:T(8,128)(2,1)}) custom-call(bf16[256,128]{1,0:T(8,128)(2,1)} %refs_0_.1, bf16[256,128]{1,0:T(8,128)(2,1)} %refs_1_.1, bf16[256,128]{1,0:T(8,128)(2,1)} %refs_2_.1, f32[1,1]{1,0:T(1,128)} %bitcast.9.refs_3_, f32[1,128]{1,0:T(1,128)} %bitcast.17, bf16[2048,128]{1,0:T(8,128)(2,1)} %refs_5_.1, ...), custom_call_target="tpu_custom_call" | custom-call | tf_op jit(solution)/shard_map/pallas_call | solution.py:838
  92.8 0.0 copy-start
  92.8 1.5 %copy.19 = bf16[256,128]{1,0:T(8,128)(2,1)} copy(bf16[256,128]{1,0:T(8,128)(2,1)} %get-tuple-element.4) | data formatting | bytes 131072
  94.3 0.0 copy-done
  94.3 0.6 copy.20
Async XLA Ops:
  92.8 1.5 %copy-start = (bf16[256,128]{1,0:T(8,128)(2,1)S(1)}, bf16[256,128]{1,0:T(8,128)(2,1)}, u32[]{:S(2)}) copy-start(bf16[256,128]{1,0:T(8,128)(2,1)} %get-tuple-element.5) | copy-start | bytes 196612

commit v4 on v3

--- a/solution.py
+++ b/solution.py
@@ -11,6 +11,72 @@
 GROUP_SIZE = 4
 LANES = 128
 CHUNKS = 4
+ORDER = (
+    ("gather", 0, 0),
+    ("inputs",),
+    ("gather", 0, 1),
+    ("gather", 1, 0),
+    ("gather", 0, 2),
+    ("gather", 0, 3),
+    ("gather", 1, 1),
+    ("chain", 1),
+    ("own",),
+    ("attend", 1),
+    ("gather", 1, 2),
+    ("gather", 2, 0),
+    ("gather", 1, 3),
+    ("far", 0),
+    ("gather", 2, 1),
+    ("chain", 2),
+    ("attend", 2),
+    ("far", 1),
+    ("gather", 2, 2),
+    ("far", 2),
+    ("gather", 3, 0),
+    ("far", 3),
+    ("expert", 0),
+    ("gather", 2, 3),
+    ("chain", 3),
+    ("attend", 3),
+    ("gather", 3, 1),
+    ("sum", 4, 0),
+    ("gather", 3, 2),
+    ("expert", 1),
+    ("gather", 3, 3),
+    ("expert", 2),
+    ("sum", 3, 0),
+    ("expert", 3),
+    ("sum", 4, 1),
+    ("sum", 4, 2),
+    ("chain", 4),
+    ("attend", 4),
+    ("attend", 5),
+    ("sum", 2, 0),
+    ("attend", 6),
+    ("sum", 3, 1),
+    ("sum", 4, 3),
+    ("sum", 3, 2),
+    ("attend", 7),
+    ("results",),
+    ("sum", 1, 0),
+    ("sum", 2, 1),
+    ("sum", 3, 3),
+    ("sum", 2, 2),
+    ("sum", 0, 0),
+    ("sum", 1, 1),
+    ("merge",),
+    ("sum", 2, 3),
+    ("sum", 1, 2),
+    ("sum", 0, 1),
+    ("heads", 1),
+    ("sum", 1, 3),
+    ("sum", 0, 2),
+    ("heads", 2),
+    ("sum", 0, 3),
+    ("heads", 3),
+    ("heads", 4),
+    ("project",),
+)
 F32 = jnp.float32
 BF16 = jnp.bfloat16
 
@@ -68,6 +134,7 @@
     pos,
     weight,
     disp,
+    disp_far,
     xs,
     parts,
     mate,
@@ -79,6 +146,8 @@
     ret,
     a_send,
     a_recv,
+    f_send,
+    f_recv,
     up_send,
     up_recv,
     dn_send,
@@ -153,6 +222,33 @@
 
         loop(0, count, one)
 
+
+    input_copies = [
+        pltpu.make_async_copy(src, dst, i_sem.at[i])
+        for i, (src, dst) in enumerate(
+            (
+                (rin_hbm, rin),
+                (ids_hbm, ids_ref),
+                (gl_hbm, gl_ref),
+                (il_hbm, il_ref),
+                (rgain_hbm, rgain_ref),
+                (q_hbm, qb.at[x]),
+                (k_hbm, kb.at[z]),
+                (v_hbm, vb.at[z]),
+                (scale_hbm, scale_ref),
+                (hgain_hbm, hgain_ref),
+            )
+        )
+    ]
+    weight_copies = [
+        pltpu.make_async_copy(src, dst, w_sem.at[i])
+        for i, (src, dst) in enumerate(
+            ((gw_hbm, gw), (uw_hbm, uw), (dw_hbm, dw), (ow_hbm, ow))
+        )
+    ]
+    for copy in input_copies:
+        copy.start()
+
     barrier = pltpu.get_barrier_semaphore()
 
     def greet(peer):
@@ -175,33 +271,7 @@
         barrier, inc=1, device_id={"c": other}, device_id_type=pl.DeviceIdType.MESH
     )
 
-    input_copies = [
-        pltpu.make_async_copy(src, dst, i_sem.at[i])
-        for i, (src, dst) in enumerate(
-            (
-                (ids_hbm, ids_ref),
-                (gl_hbm, gl_ref),
-                (il_hbm, il_ref),
-                (rgain_hbm, rgain_ref),
-                (rin_hbm, rin),
-                (q_hbm, qb.at[x]),
-                (k_hbm, kb.at[z]),
-                (v_hbm, vb.at[z]),
-                (scale_hbm, scale_ref),
-                (hgain_hbm, hgain_ref),
-            )
-        )
-    ]
-    weight_copies = [
-        pltpu.make_async_copy(src, dst, w_sem.at[i])
-        for i, (src, dst) in enumerate(
-            ((gw_hbm, gw), (uw_hbm, uw), (dw_hbm, dw), (ow_hbm, ow))
-        )
-    ]
-    for copy in input_copies + weight_copies:
-        copy.start()
-
-    for copy in input_copies[:4]:
+    for copy in input_copies[1:5]:
         copy.wait()
     ids = ids_ref[...]
     shape = (nep, rows)
@@ -234,16 +304,26 @@
         slots = lax.broadcasted_iota(jnp.int32, (total, rows), 0).astype(F32)
         return jnp.where(pos[i : i + 1, :] == slots, 1.0, 0.0).astype(BF16)
 
-    own_cols = pl.ds(pl.multiple_of(t * LANES, LANES), LANES)
-    input_copies[4].wait()
+    input_copies[0].wait()
     source = rin[...].astype(F32)
     inv = lax.rsqrt(jnp.sum(source * source, axis=-1, keepdims=True) * (1.0 / width) + EPSILON)
-    normed = (rin[:, own_cols].astype(F32) * inv * rgain_ref[:, own_cols]).astype(BF16)
-    disp[...] = jnp.dot(
-        one_hot(0) + one_hot(1), normed, preferred_element_type=F32
+
+    def normed(block):
+        columns = pl.ds(pl.multiple_of((block * 2 + c) * LANES, LANES), LANES)
+        return (rin[:, columns].astype(F32) * inv * rgain_ref[:, columns]).astype(BF16)
+
+    y_far = y_at(half_ring)
+    spread = jnp.dot(
+        one_hot(0) + one_hot(1),
+        jnp.concatenate([normed(y), normed(y_far)], axis=1),
+        preferred_element_type=F32,
     ).astype(BF16)
+    disp[...] = spread[:, :LANES]
+    disp_far[...] = spread[:, LANES:]
     for copy in input_copies[5:]:
         copy.wait()
+    for copy in weight_copies:
+        copy.start()
 
     pl.semaphore_wait(barrier, nep - 1 + ny - 1 + 1)
 
@@ -260,9 +340,20 @@
             x=lax.rem(peer, nx),
         )
 
+    def dispatch_far(peer):
+        return remote(
+            disp_far.at[slot_rows(peer)],
+            xs.at[y_far, c, slot_rows(e)],
+            f_send.at[peer],
+            f_recv.at[e],
+            z=peer // nx,
+            x=lax.rem(peer, nx),
+        )
+
     for j in range(CHUNKS):
         each_other(nearby(j) * per_chunk, per_chunk, lambda peer: dispatch(peer).start())
     xs[y, c, slot_rows(e), :] = disp[slot_rows(e), :]
+    xs[y_far, c, slot_rows(e), :] = disp_far[slot_rows(e), :]
 
     def query_copy(r):
         return remote(
@@ -291,6 +382,8 @@
 
     def send_queries_and_keys():
         chain_send(1)
+        for j in range(CHUNKS):
+            each_other(nearby(j) * per_chunk, per_chunk, lambda peer: dispatch_far(peer).start())
         for r in range(reach + 1, nz):
 
             @pl.when(z + r < nz)
@@ -388,50 +481,36 @@
     def chunk_rows(k):
         return pl.ds(pl.multiple_of(k * chunk, chunk), chunk)
 
-    def upper_rows(k):
-        return pl.ds(pl.multiple_of(k * chunk, half), half)
-
-    def lower_rows(k):
-        return pl.ds(pl.multiple_of(k * chunk + half, half), half)
-
     def up_copy(s, k):
-        where = upper_rows(k) if s == half_ring - 1 else chunk_rows(k)
+        where = chunk_rows(k)
         block = xs.at[y_at(-s), c, where]
         return remote(block, block, up_send.at[k, s], up_recv.at[k, s], y=y_next)
 
     def dn_copy(s, k):
-        where = lower_rows(k) if s == half_ring - 1 else chunk_rows(k)
+        where = chunk_rows(k)
         block = xs.at[y_at(s), c, where]
         return remote(block, block, dn_send.at[k, s], dn_recv.at[k, s], y=y_prev)
 
     def up_arrival(s, k):
-        where = upper_rows(k) if s == half_ring - 1 else chunk_rows(k)
+        where = chunk_rows(k)
         block = xs.at[y_at(-s - 1), c, where]
         return remote(block, block, up_send.at[k, s], up_recv.at[k, s], y=y_next)
 
     def dn_arrival(s, k):
-        where = lower_rows(k) if s == half_ring - 1 else chunk_rows(k)
+        where = chunk_rows(k)
         block = xs.at[y_at(s + 1), c, where]
         return remote(block, block, dn_send.at[k, s], dn_recv.at[k, s], y=y_prev)
 
-    def mate_blocks(k, core):
-        blocks = [xs.at[y, core, chunk_rows(k)]]
-        for s in range(half_ring):
-            last = s == half_ring - 1
-            blocks.append(
-                xs.at[y_at(-s - 1), core, upper_rows(k) if last else chunk_rows(k)]
-            )
-            blocks.append(
-                xs.at[y_at(s + 1), core, lower_rows(k) if last else chunk_rows(k)]
-            )
-        return blocks
+    def mate_block(number, k, core):
+        shift = (0, -1, 1, -2, 2, -3, 3, half_ring)[number]
+        return xs.at[y_at(shift), core, chunk_rows(k)]
 
     def mate_copy(number, k):
-        block = mate_blocks(k, c)[number]
+        block = mate_block(number, k, c)
         return remote(block, block, m_send.at[k, number], m_recv.at[k, number], c=other)
 
     def mate_arrival(number, k):
-        block = mate_blocks(k, other)[number]
+        block = mate_block(number, k, other)
         return remote(block, block, m_send.at[k, number], m_recv.at[k, number], c=other)
 
     def first_sends(k):
@@ -442,13 +521,27 @@
 
     def pass_on(s, k):
         up_arrival(s, k).wait_recv()
-        if s + 1 < half_ring:
+        if s + 2 < half_ring:
             up_copy(s + 1, k).start()
         mate_copy(2 * s + 1, k).start()
         dn_arrival(s, k).wait_recv()
-        if s + 1 < half_ring:
+        if s + 2 < half_ring:
             dn_copy(s + 1, k).start()
         mate_copy(2 * s + 2, k).start()
+
+    def far_rows(k):
+        def wait_far(peer):
+            remote(
+                disp_far.at[slot_rows(0)],
+                xs.at[y_far, c, slot_rows(peer)],
+                f_send.at[peer],
+                f_recv.at[peer],
+                z=z,
+                x=x,
+            ).wait_recv()
+
+        each_other(k * per_chunk, per_chunk, wait_far)
+        mate_copy(ny - 1, k).start()
 
     def result_copies(r):
         to_x = lax.rem(x + r, nx)
@@ -473,7 +566,7 @@
         stat_in[x] = stat[x]
 
     def expert(k):
-        for number in range(2 * half_ring + 1):
+        for number in range(ny):
             mate_arrival(number, k).wait_recv()
         gate = jnp.zeros((chunk, gw.shape[1]), F32)
         up = jnp.zeros((chunk, gw.shape[1]), F32)
@@ -549,18 +642,9 @@
     def answer(k):
         sum_up(k, 1).wait_recv()
         sum_dn(k, 1).wait_recv()
-        if half_ring > 1:
-            ans[chunk_rows(k), :] = (
-                chip_sum(k, y, full) + rb_up[k, 0].astype(F32) + rb_dn[k, 0].astype(F32)
-            ).astype(BF16)
-        else:
-            ans[upper_rows(k), :] = (
-                chip_sum(k, y, top) + rb_up[k, 0, top].astype(F32)
-            ).astype(BF16)
-            ans[lower_rows(k), :] = (
-                chip_sum(k, y, bottom) + rb_dn[k, 0, bottom].astype(F32)
-            ).astype(BF16)
-
+        ans[chunk_rows(k), :] = (
+            chip_sum(k, y, full) + rb_up[k, 0].astype(F32) + rb_dn[k, 0].astype(F32)
+        ).astype(BF16)
         each_other(k * per_chunk, per_chunk, lambda target: back_copy(target).start())
 
     def back_copy(target):
@@ -634,34 +718,44 @@
         head_dn(0, 0).start()
         head_mate(0, c).start()
 
-    stages = [first_sends]
-    stages += [lambda k, s=s: pass_on(s, k) for s in range(half_ring)]
-    stages += [expert, first_sum]
-    stages += [lambda k, d=d: sum_step(k, d) for d in range(half_ring - 1, 0, -1)]
-    stages += [answer]
-    beside = {
-        0: [send_queries_and_keys],
-        2: [lambda: chain_step(1), own_attention],
-        3: [lambda: chain_step(2), lambda: attend_far(1)],
-        4: [lambda: chain_step(3), lambda: attend_far(2)],
-        5: [lambda: chain_step(4), lambda: attend_far(3)],
-        6: [lambda: attend_far(4), lambda: attend_far(5)],
-        7: [lambda: attend_far(6), lambda: attend_far(7), send_results],
-        9: [merge],
-        10: [lambda: head_pass(0)],
-        11: [lambda: head_pass(1)],
-        12: [lambda: head_pass(2)],
-        13: [lambda: head_pass(3)],
+    def weights_and_expert(k):
+        if not weights_here:
+            weights_here.append(True)
+            for copy in weight_copies[:3]:
+                copy.wait()
+        expert(k)
+
+    def sum_stage(d, k):
+        if d == half_ring:
+            first_sum(k)
+        elif d > 0:
+            sum_step(k, d)
+        else:
+            answer(k)
+
+    def gather_stage(s, k):
+        if s == 0:
+            first_sends(k)
+        else:
+            pass_on(s - 1, k)
+
+    weights_here = []
+    stages = {
+        "gather": lambda s, j: gather_stage(s, nearby(j)),
+        "inputs": send_queries_and_keys,
+        "far": lambda j: far_rows(nearby(j)),
+        "chain": chain_step,
+        "own": own_attention,
+        "attend": attend_far,
+        "expert": lambda j: weights_and_expert(nearby(j)),
+        "sum": lambda d, j: sum_stage(d, nearby(j)),
+        "results": send_results,
+        "merge": merge,
+        "heads": lambda s: head_pass(s - 1),
+        "project": lambda: None,
     }
-    for wave in range(len(stages) + CHUNKS - 1):
-        for j in range(CHUNKS):
-            if 0 <= wave - j < len(stages):
-                if wave - j == half_ring + 1 and j == 0:
-                    for copy in weight_copies[:3]:
-                        copy.wait()
-                stages[wave - j](nearby(j))
-        for work in beside.get(wave, []):
-            work()
+    for stage in ORDER:
+        stages[stage[0]](*stage[1:])
     ret[slot_rows(e), :] = ans[slot_rows(e), :]
 
     weight_copies[3].wait()
@@ -695,17 +789,19 @@
 
     def drain(peer):
         dispatch(peer).wait_send()
+        dispatch_far(peer).wait_send()
         back_copy(peer).wait_send()
 
     each_other(0, nep, drain)
 
     def drain_chunk(k):
-        for s in range(half_ring):
+        for s in range(half_ring - 1):
             up_copy(s, k).wait_send()
             dn_copy(s, k).wait_send()
-            sum_up(k, s + 1).wait_send()
-            sum_dn(k, s + 1).wait_send()
-        for number in range(2 * half_ring + 1):
+        for d in range(1, half_ring + 1):
+            sum_up(k, d).wait_send()
+            sum_dn(k, d).wait_send()
+        for number in range(ny):
             mate_copy(number, k).wait_send()
         part_copy(k).wait_send()
 
@@ -781,6 +877,7 @@
         vmem((8, rows), F32),
         vmem((8, rows), F32),
         vmem((total, LANES), BF16),
+        vmem((total, LANES), BF16),
         vmem((ny, 2, total, LANES), BF16),
         vmem((CHUNKS, 2, ny, chunk, LANES), BF16),
         vmem((CHUNKS, ny, chunk, LANES), BF16),
@@ -790,6 +887,8 @@
         vmem((CHUNKS, half_ring, chunk, LANES), BF16),
         vmem((total, LANES), BF16),
         vmem((total, LANES), BF16),
+        dma((nep,)),
+        dma((nep,)),
         dma((nep,)),
         dma((nep,)),
         dma((CHUNKS, half_ring)),

time: 95.1 us -> 88.7 us (0.933)
  the two profiles are of different devices: /device:TPU:8 before, /device:TPU:64 now
where the time goes in v4:
time: 88.7 us; the launch traced here: 88.5 us
  Pallas kernels  85 us (96%)
  local copies, waits for them, and re-layouts  2.14 us (2%)
  between operations  1.3 us (1%)
    pallas_call x1, Pallas kernels, local(): pl.pallas_call(lambda *refs: kernel(sizes, *refs), out_shape=(jax.ShapeDt...  85 us
    unnamed x4, local copies, waits for them, and re-layouts  2.14 us

profile of v4, /device:TPU:64, one launch (start us, length us, event | category | flops | bytes accessed | tf_op | source)
XLA Modules:
  0.0 88.5 jit_solution(14187828264212108123)
XLA Ops:
  1.3 85.0 %shard_map.149 = (bf16[256,128]{1,0:T(8,128)(2,1)}, bf16[256,128]{1,0:T(8,128)(2,1)}) custom-call(bf16[256,128]{1,0:T(8,128)(2,1)} %refs_0_.1, bf16[256,128]{1,0:T(8,128)(2,1)} %refs_1_.1, bf16[256,128]{1,0:T(8,128)(2,1)} %refs_2_.1, f32[1,1]{1,0:T(1,128)} %bitcast.9.refs_3_, f32[1,128]{1,0:T(1,128)} %bitcast.17, bf16[2048,128]{1,0:T(8,128)(2,1)} %refs_5_.1, ...), custom_call_target="tpu_custom_call" | custom-call | tf_op jit(solution)/shard_map/pallas_call | solution.py:937
  86.3 0.0 copy-start
  86.3 1.5 %copy.19 = bf16[256,128]{1,0:T(8,128)(2,1)} copy(bf16[256,128]{1,0:T(8,128)(2,1)} %get-tuple-element.4) | data formatting | bytes 131072
  87.8 0.0 copy-done
  87.8 0.6 copy.20
Async XLA Ops:
  86.3 1.5 %copy-start = (bf16[256,128]{1,0:T(8,128)(2,1)S(1)}, bf16[256,128]{1,0:T(8,128)(2,1)}, u32[]{:S(2)}) copy-start(bf16[256,128]{1,0:T(8,128)(2,1)} %get-tuple-element.5) | copy-start | bytes 196612

commit v5 on v4

--- a/solution.py
+++ b/solution.py
@@ -18,60 +18,61 @@
     ("gather", 1, 0),
     ("gather", 0, 2),
     ("gather", 0, 3),
+    ("own",),
     ("gather", 1, 1),
     ("chain", 1),
-    ("own",),
+    ("keys",),
+    ("gather", 2, 0),
     ("attend", 1),
     ("gather", 1, 2),
-    ("gather", 2, 0),
     ("gather", 1, 3),
     ("far", 0),
     ("gather", 2, 1),
+    ("far", 1),
+    ("gather", 3, 0),
     ("chain", 2),
     ("attend", 2),
-    ("far", 1),
     ("gather", 2, 2),
+    ("expert", 0),
+    ("far", 3),
+    ("gather", 2, 3),
     ("far", 2),
-    ("gather", 3, 0),
-    ("far", 3),
-    ("expert", 0),
-    ("gather", 2, 3),
-    ("chain", 3),
-    ("attend", 3),
     ("gather", 3, 1),
     ("sum", 4, 0),
+    ("expert", 1),
+    ("chain", 3),
     ("gather", 3, 2),
-    ("expert", 1),
+    ("attend", 3),
     ("gather", 3, 3),
+    ("sum", 4, 1),
     ("expert", 2),
+    ("expert", 3),
     ("sum", 3, 0),
-    ("expert", 3),
-    ("sum", 4, 1),
     ("sum", 4, 2),
+    ("sum", 3, 1),
     ("chain", 4),
     ("attend", 4),
     ("attend", 5),
     ("sum", 2, 0),
     ("attend", 6),
-    ("sum", 3, 1),
-    ("sum", 4, 3),
-    ("sum", 3, 2),
     ("attend", 7),
     ("results",),
+    ("sum", 4, 3),
+    ("sum", 2, 1),
     ("sum", 1, 0),
-    ("sum", 2, 1),
+    ("sum", 3, 2),
     ("sum", 3, 3),
+    ("sum", 1, 1),
+    ("sum", 0, 0),
+    ("merge",),
     ("sum", 2, 2),
-    ("sum", 0, 0),
-    ("sum", 1, 1),
-    ("merge",),
     ("sum", 2, 3),
-    ("sum", 1, 2),
     ("sum", 0, 1),
     ("heads", 1),
+    ("sum", 1, 2),
     ("sum", 1, 3),
+    ("heads", 2),
     ("sum", 0, 2),
-    ("heads", 2),
     ("sum", 0, 3),
     ("heads", 3),
     ("heads", 4),
@@ -116,8 +117,7 @@
     gw_hbm,
     uw_hbm,
     dw_hbm,
-    mix_ref,
-    rout_ref,
+    out_ref,
     gw,
     uw,
     dw,
@@ -251,25 +251,19 @@
 
     barrier = pltpu.get_barrier_semaphore()
 
-    def greet(peer):
+    def greet(**where):
         pl.semaphore_signal(
-            barrier,
-            inc=1,
-            device_id={"z": peer // nx, "x": lax.rem(peer, nx)},
-            device_id_type=pl.DeviceIdType.MESH,
-        )
-
-    each_other(0, nep, greet)
-
-    def greet_y(r):
-        pl.semaphore_signal(
-            barrier, inc=1, device_id={"y": lax.rem(y + r, ny)}, device_id_type=pl.DeviceIdType.MESH
-        )
-
-    loop(1, ny, greet_y)
-    pl.semaphore_signal(
-        barrier, inc=1, device_id={"c": other}, device_id_type=pl.DeviceIdType.MESH
-    )
+            barrier, inc=1, device_id=where, device_id_type=pl.DeviceIdType.MESH
+        )
+
+    near_z = [lax.rem(z + d, nz) for d in range(nz)]
+    near_x = [lax.rem(x + d, nx) for d in range(nx)]
+    apart = [(i, j) for i in range(nz) for j in range(nx) if i + j > 0]
+    for i, j in sorted(apart, key=lambda ij: -min(ij[0], nz - ij[0]) - min(ij[1], nx - ij[1])):
+        greet(z=near_z[i], x=near_x[j])
+    greet(y=y_next)
+    greet(y=y_prev)
+    greet(c=other)
 
     for copy in input_copies[1:5]:
         copy.wait()
@@ -325,7 +319,7 @@
     for copy in weight_copies:
         copy.start()
 
-    pl.semaphore_wait(barrier, nep - 1 + ny - 1 + 1)
+    pl.semaphore_wait(barrier, nep - 1 + 2 + 1)
 
     def slot_rows(index):
         return pl.ds(pl.multiple_of(index * cap, cap), cap)
@@ -380,10 +374,14 @@
             for copy in chain_copies(r):
                 copy.start()
 
-    def send_queries_and_keys():
+    def send_inputs():
+        for r in range(1, nx):
+            query_copy(r).start()
         chain_send(1)
         for j in range(CHUNKS):
             each_other(nearby(j) * per_chunk, per_chunk, lambda peer: dispatch_far(peer).start())
+
+    def send_far_keys():
         for r in range(reach + 1, nz):
 
             @pl.when(z + r < nz)
@@ -391,9 +389,6 @@
                 for copy in far_copies(r):
                     copy.start()
 
-        for r in range(1, nx):
-            query_copy(r).start()
-
     maps = 2 * rows
     qk = LANES // 2
     keep_low = lax.broadcasted_iota(jnp.int32, (rows, LANES), 1) < qk
@@ -404,9 +399,12 @@
         qs[index, rows:maps, :] = jnp.where(keep_low, 0.0, scaled).astype(BF16)
 
     def attend(key_block, value_block, masked):
+        keys = key_block[...]
+        values = value_block[...].T
+
         def one(index):
             scores = lax.dot_general(
-                key_block[...],
+                keys,
                 qs[index],
                 (((1,), (1,)), ((), ())),
                 preferred_element_type=F32,
@@ -429,18 +427,14 @@
                     terms, axis=0, keepdims=True
                 )
             stat[index, 0:1, :] = new_max
-            weighted = lax.dot_general(
-                value_block[...],
-                terms.astype(BF16),
-                (((0,), (0,)), ((), ())),
-                preferred_element_type=F32,
-            )
+            weighted = jnp.dot(values, terms.astype(BF16), preferred_element_type=F32)
             if masked:
                 acc[index] = weighted
             else:
                 acc[index] = acc[index] * factor + weighted
 
-        loop(0, nx, one)
+        for index in range(nx):
+            one(index)
 
     def own_attention():
         stack_query(qb[x], x)
@@ -742,7 +736,8 @@
     weights_here = []
     stages = {
         "gather": lambda s, j: gather_stage(s, nearby(j)),
-        "inputs": send_queries_and_keys,
+        "inputs": send_inputs,
+        "keys": send_far_keys,
         "far": lambda j: far_rows(nearby(j)),
         "chain": chain_step,
         "own": own_attention,
@@ -767,30 +762,11 @@
         mixed += jnp.dot(
             both, ow[block * 2 * LANES : (block + 1) * 2 * LANES, :], preferred_element_type=F32
         )
-    mix_ref[...] = mixed.astype(BF16)
-
-    def wait_back(peer):
-        remote(
-            ans.at[slot_rows(0)],
-            ret.at[slot_rows(peer)],
-            b_send.at[peer],
-            b_recv.at[peer],
-            z=z,
-            x=x,
-        ).wait_recv()
-
-    each_other(0, nep, wait_back)
-    routed = jnp.zeros((LANES, rows), F32)
-    for i in range(2):
-        routed += weight[i : i + 1, :] * lax.dot_general(
-            ret[...], one_hot(i), (((0,), (0,)), ((), ())), preferred_element_type=F32
-        )
-    rout_ref[...] = routed.T.astype(BF16)
+    out_ref[0] = mixed.astype(BF16)
 
     def drain(peer):
         dispatch(peer).wait_send()
         dispatch_far(peer).wait_send()
-        back_copy(peer).wait_send()
 
     each_other(0, nep, drain)
 
@@ -829,6 +805,26 @@
         head_dn(s, 0).wait_send()
     for number in range(2 * half_ring + 1):
         head_mate(number, c).wait_send()
+
+    def wait_back(peer):
+        remote(
+            ans.at[slot_rows(0)],
+            ret.at[slot_rows(peer)],
+            b_send.at[peer],
+            b_recv.at[peer],
+            z=z,
+            x=x,
+        ).wait_recv()
+
+    each_other(0, nep, wait_back)
+    routed = jnp.zeros((LANES, rows), F32)
+    for i in range(2):
+        routed += weight[i : i + 1, :] * lax.dot_general(
+            ret[...], one_hot(i), (((0,), (0,)), ((), ())), preferred_element_type=F32
+        )
+    out_ref[1] = routed.T.astype(BF16)
+
+    each_other(0, nep, lambda peer: back_copy(peer).wait_send())
 
 
 def local(
@@ -934,14 +930,11 @@
     ]
     whole = pl.BlockSpec(memory_space=pltpu.VMEM)
     far = pl.BlockSpec(memory_space=pl.ANY)
-    return pl.pallas_call(
+    both = pl.pallas_call(
         lambda *refs: kernel(sizes, *refs),
-        out_shape=(
-            jax.ShapeDtypeStruct((rows, LANES), BF16),
-            jax.ShapeDtypeStruct((rows, LANES), BF16),
-        ),
+        out_shape=jax.ShapeDtypeStruct((2, rows, LANES), BF16),
         in_specs=[far] * 14,
-        out_specs=(whole, whole),
+        out_specs=whole,
         scratch_shapes=scratch,
         compiler_params=pltpu.CompilerParams(
             collective_id=0, has_side_effects=True, vmem_limit_bytes=60 * 1024 * 1024
@@ -962,6 +955,7 @@
         up_weight[0],
         down_weight[0],
     )
+    return both[0], both[1]
 
 
 def build(mesh, sizes):

time: 88.7 us -> 83.9 us (0.946)
  the two profiles are of different devices: /device:TPU:64 before, /device:TPU:1 now
where the time goes in v5:
time: 83.9 us; the launch traced here: 83.7 us
  Pallas kernels  80.8 us (96%)
  local copies, waits for them, and re-layouts  1.53 us (2%)
  between operations  1.29 us (2%)
    pallas_call x1, Pallas kernels, local(): pl.pallas_call(lambda *refs: kernel(sizes, *refs), out_shape=jax.ShapeDty...  80.8 us

profile of v5, /device:TPU:1, one launch (start us, length us, event | category | flops | bytes accessed | tf_op | source)
XLA Modules:
  0.0 83.7 jit_solution(15209634561420944163)
XLA Ops:
  1.3 80.8 %shard_map.149 = bf16[2,256,128]{2,1,0:T(8,128)(2,1)} custom-call(bf16[256,128]{1,0:T(8,128)(2,1)} %refs_0_.1, bf16[256,128]{1,0:T(8,128)(2,1)} %refs_1_.1, bf16[256,128]{1,0:T(8,128)(2,1)} %refs_2_.1, f32[1,1]{1,0:T(1,128)} %bitcast.13.refs_3_, f32[1,128]{1,0:T(1,128)} %bitcast.21, bf16[2048,128]{1,0:T(8,128)(2,1)} %refs_5_.1, bf16[256,2048]{1,0:T(8,128)(2,1)} %refs_6_.1, ...), custom_call_target="tpu_custom_call" | custom-call | tf_op jit(solution)/shard_map/pallas_call | solution.py:933
  82.1 1.5 %slice_bitcast_fusion = (bf16[256,128]{1,0:T(8,128)(2,1)}, bf16[256,128]{1,0:T(8,128)(2,1)}) fusion(bf16[2,256,128]{2,1,0:T(8,128)(2,1)} %shard_map.149), kind=kLoop, calls=%fused_computation | loop fusion | bytes 262144 | tf_op jit(solution)/shard_map/squeeze | solution.py:958

commit v6 on v5

--- a/solution.py
+++ b/solution.py
@@ -10,7 +10,7 @@
 LOWEST = -1e30
 GROUP_SIZE = 4
 LANES = 128
-CHUNKS = 4
+CHUNKS = 8
 ORDER = (
     ("gather", 0, 0),
     ("inputs",),
@@ -18,62 +18,106 @@
     ("gather", 1, 0),
     ("gather", 0, 2),
     ("gather", 0, 3),
+    ("gather", 1, 1),
+    ("gather", 0, 4),
+    ("gather", 2, 0),
+    ("gather", 0, 5),
     ("own",),
-    ("gather", 1, 1),
+    ("gather", 1, 3),
     ("chain", 1),
     ("keys",),
-    ("gather", 2, 0),
+    ("gather", 1, 2),
+    ("gather", 0, 7),
+    ("gather", 2, 1),
     ("attend", 1),
-    ("gather", 1, 2),
-    ("gather", 1, 3),
+    ("gather", 1, 4),
+    ("gather", 3, 0),
+    ("gather", 0, 6),
+    ("gather", 1, 5),
+    ("gather", 2, 3),
     ("far", 0),
-    ("gather", 2, 1),
+    ("gather", 2, 2),
     ("far", 1),
-    ("gather", 3, 0),
+    ("gather", 1, 7),
+    ("expert", 0),
+    ("far", 2),
+    ("gather", 3, 1),
     ("chain", 2),
     ("attend", 2),
-    ("gather", 2, 2),
-    ("expert", 0),
+    ("sum", 4, 0),
     ("far", 3),
-    ("gather", 2, 3),
-    ("far", 2),
-    ("gather", 3, 1),
-    ("sum", 4, 0),
+    ("gather", 2, 4),
+    ("far", 4),
     ("expert", 1),
+    ("gather", 1, 6),
+    ("far", 5),
+    ("gather", 3, 3),
+    ("gather", 2, 5),
+    ("far", 6),
+    ("far", 7),
+    ("gather", 3, 2),
+    ("sum", 4, 1),
+    ("expert", 3),
+    ("gather", 2, 7),
+    ("sum", 3, 0),
+    ("expert", 2),
+    ("gather", 3, 4),
     ("chain", 3),
-    ("gather", 3, 2),
+    ("sum", 4, 3),
     ("attend", 3),
-    ("gather", 3, 3),
-    ("sum", 4, 1),
-    ("expert", 2),
-    ("expert", 3),
-    ("sum", 3, 0),
     ("sum", 4, 2),
     ("sum", 3, 1),
+    ("expert", 4),
+    ("gather", 3, 7),
+    ("gather", 3, 5),
+    ("gather", 2, 6),
+    ("sum", 2, 0),
+    ("sum", 3, 3),
+    ("expert", 7),
+    ("expert", 5),
+    ("sum", 2, 1),
+    ("sum", 3, 2),
+    ("sum", 4, 4),
+    ("sum", 4, 7),
+    ("gather", 3, 6),
     ("chain", 4),
     ("attend", 4),
+    ("sum", 1, 0),
+    ("sum", 2, 3),
     ("attend", 5),
-    ("sum", 2, 0),
     ("attend", 6),
+    ("sum", 3, 4),
     ("attend", 7),
     ("results",),
-    ("sum", 4, 3),
-    ("sum", 2, 1),
-    ("sum", 1, 0),
-    ("sum", 3, 2),
-    ("sum", 3, 3),
+    ("sum", 3, 7),
+    ("sum", 1, 3),
+    ("sum", 2, 2),
+    ("sum", 0, 0),
+    ("expert", 6),
+    ("sum", 4, 5),
+    ("sum", 2, 4),
     ("sum", 1, 1),
-    ("sum", 0, 0),
+    ("sum", 4, 6),
+    ("sum", 2, 7),
+    ("sum", 0, 3),
+    ("sum", 1, 2),
+    ("sum", 3, 5),
+    ("sum", 1, 4),
+    ("sum", 0, 1),
+    ("sum", 3, 6),
     ("merge",),
-    ("sum", 2, 2),
-    ("sum", 2, 3),
-    ("sum", 0, 1),
+    ("sum", 1, 7),
+    ("sum", 0, 2),
+    ("sum", 2, 5),
+    ("sum", 0, 4),
+    ("sum", 2, 6),
     ("heads", 1),
-    ("sum", 1, 2),
-    ("sum", 1, 3),
+    ("sum", 0, 7),
+    ("sum", 1, 5),
+    ("sum", 1, 6),
     ("heads", 2),
-    ("sum", 0, 2),
-    ("sum", 0, 3),
+    ("sum", 0, 5),
+    ("sum", 0, 6),
     ("heads", 3),
     ("heads", 4),
     ("project",),
@@ -164,8 +208,7 @@
     b_recv,
     qb,
     qs,
-    kb,
-    vb,
+    kvb,
     acc,
     stat,
     o_out,
@@ -176,8 +219,6 @@
     q_recv,
     k_send,
     k_recv,
-    v_send,
-    v_recv,
     o_send,
     o_recv,
     s_send,
@@ -212,7 +253,13 @@
     group = z // (nz // CHUNKS)
 
     def nearby(j):
-        return lax.rem(group + (0, 1, 3, 2)[j], CHUNKS)
+        return lax.rem(group + (0, 1, 7, 2, 6, 3, 5, 4)[j], CHUNKS)
+
+    def wait_sent(block, sem):
+        remote(block, block, sem, sem, c=other).wait_send()
+
+    def wait_arrived(block, sem):
+        remote(block, block, sem, sem, c=other).wait_recv()
 
     def each_other(first, count, body):
         def one(i):
@@ -233,8 +280,8 @@
                 (il_hbm, il_ref),
                 (rgain_hbm, rgain_ref),
                 (q_hbm, qb.at[x]),
-                (k_hbm, kb.at[z]),
-                (v_hbm, vb.at[z]),
+                (k_hbm, kvb.at[z, 0]),
+                (v_hbm, kvb.at[z, 1]),
                 (scale_hbm, scale_ref),
                 (hgain_hbm, hgain_ref),
             )
@@ -328,8 +375,8 @@
         return remote(
             disp.at[slot_rows(peer)],
             xs.at[y, c, slot_rows(e)],
-            a_send.at[peer],
-            a_recv.at[e],
+            a_send.at[0],
+            a_recv.at[group],
             z=peer // nx,
             x=lax.rem(peer, nx),
         )
@@ -338,8 +385,8 @@
         return remote(
             disp_far.at[slot_rows(peer)],
             xs.at[y_far, c, slot_rows(e)],
-            f_send.at[peer],
-            f_recv.at[e],
+            f_send.at[0],
+            f_recv.at[group],
             z=peer // nx,
             x=lax.rem(peer, nx),
         )
@@ -351,28 +398,24 @@
 
     def query_copy(r):
         return remote(
-            qb.at[x], qb.at[x], q_send.at[r], q_recv.at[r], x=lax.rem(x + r, nx)
+            qb.at[x], qb.at[x], q_send.at[0], q_recv.at[0], x=lax.rem(x + r, nx)
         )
 
     reach = nz // 2
 
-    def key_copies(block, r, to_z):
-        return (
-            remote(kb.at[block], kb.at[block], k_send.at[r], k_recv.at[r], z=to_z),
-            remote(vb.at[block], vb.at[block], v_send.at[r], v_recv.at[r], z=to_z),
-        )
-
-    def chain_copies(r):
-        return key_copies(jnp.maximum(z - r + 1, 0), r, jnp.minimum(z + 1, nz - 1))
-
-    def far_copies(r):
-        return key_copies(z, r, lax.rem(z + r, nz))
+    def key_copy(block, r, to_z):
+        return remote(kvb.at[block], kvb.at[block], k_send.at[r], k_recv.at[r], z=to_z)
+
+    def chain_copy(r):
+        return key_copy(jnp.maximum(z - r + 1, 0), r, jnp.minimum(z + 1, nz - 1))
+
+    def far_copy(r):
+        return key_copy(z, r, lax.rem(z + r, nz))
 
     def chain_send(r):
         @pl.when((z + 1 < nz) & (z - r + 1 >= 0))
         def _():
-            for copy in chain_copies(r):
-                copy.start()
+            chain_copy(r).start()
 
     def send_inputs():
         for r in range(1, nx):
@@ -386,8 +429,7 @@
 
             @pl.when(z + r < nz)
             def _(r=r):
-                for copy in far_copies(r):
-                    copy.start()
+                far_copy(r).start()
 
     maps = 2 * rows
     qk = LANES // 2
@@ -398,58 +440,61 @@
         qs[index, 0:rows, :] = jnp.where(keep_low, scaled, 0.0).astype(BF16)
         qs[index, rows:maps, :] = jnp.where(keep_low, 0.0, scaled).astype(BF16)
 
+    pieces = [(i, j * LANES) for i in range(nx) for j in range(maps // LANES)]
+
     def attend(key_block, value_block, masked):
         keys = key_block[...]
         values = value_block[...].T
 
-        def one(index):
-            scores = lax.dot_general(
+        def score(index, first):
+            return lax.dot_general(
                 keys,
-                qs[index],
+                qs[index, first : first + LANES, :],
                 (((1,), (1,)), ((), ())),
                 preferred_element_type=F32,
             )
+
+        ahead = score(*pieces[0])
+        for number, (index, first) in enumerate(pieces):
+            scores = ahead
+            if number + 1 < len(pieces):
+                ahead = score(*pieces[number + 1])
+            columns = slice(first, first + LANES)
             if masked:
                 key_pos = x * rows + lax.broadcasted_iota(jnp.int32, scores.shape, 0)
-                column = lax.broadcasted_iota(jnp.int32, scores.shape, 1)
-                query_pos = index * rows + jnp.where(column >= rows, column - rows, column)
+                query_pos = lax.broadcasted_iota(jnp.int32, scores.shape, 1) + (
+                    index * rows + first % rows
+                )
                 visible = query_pos >= key_pos
                 scores = jnp.where(visible, scores, LOWEST)
                 new_max = jnp.max(scores, axis=0, keepdims=True)
                 terms = jnp.where(visible, jnp.exp(scores - new_max), 0.0)
-                stat[index, 1:2, :] = jnp.sum(terms, axis=0, keepdims=True)
             else:
-                old_max = stat[index, 0:1, :]
+                old_max = stat[index, 0:1, columns]
                 new_max = jnp.maximum(old_max, jnp.max(scores, axis=0, keepdims=True))
                 terms = jnp.exp(scores - new_max)
                 factor = jnp.exp(old_max - new_max)
-                stat[index, 1:2, :] = stat[index, 1:2, :] * factor + jnp.sum(
-                    terms, axis=0, keepdims=True
-                )
-            stat[index, 0:1, :] = new_max
+            total_terms = jnp.sum(terms, axis=0, keepdims=True)
             weighted = jnp.dot(values, terms.astype(BF16), preferred_element_type=F32)
             if masked:
-                acc[index] = weighted
+                stat[index, 1:2, columns] = total_terms
+                acc[index, :, columns] = weighted
             else:
-                acc[index] = acc[index] * factor + weighted
-
+                stat[index, 1:2, columns] = stat[index, 1:2, columns] * factor + total_terms
+                acc[index, :, columns] = acc[index, :, columns] * factor + weighted
+            stat[index, 0:1, columns] = new_max
+
+    def own_attention():
+        wait_arrived(qb.at[pl.ds(0, nx - 1)], q_recv.at[0])
         for index in range(nx):
-            one(index)
-
-    def own_attention():
-        stack_query(qb[x], x)
-        for r in range(1, nx):
-            query_copy(r).wait_recv()
-            from_x = lax.rem(x + nx - r, nx)
-            stack_query(qb[from_x], from_x)
+            stack_query(qb[index], index)
         stat[...] = jnp.zeros_like(stat)
-        attend(kb.at[z], vb.at[z], True)
+        attend(kvb.at[z, 0], kvb.at[z, 1], True)
 
     def chain_step(r):
         @pl.when(z >= r)
         def _():
-            for copy in key_copies(jnp.maximum(z - r, 0), r, z):
-                copy.wait_recv()
+            key_copy(jnp.maximum(z - r, 0), r, z).wait_recv()
             if r < reach:
                 chain_send(r + 1)
 
@@ -458,19 +503,14 @@
         def _():
             from_z = jnp.maximum(z - r, 0)
             if r > reach:
-                for copy in key_copies(from_z, r, z):
-                    copy.wait_recv()
-            attend(kb.at[from_z], vb.at[from_z], False)
-
-    def wait_dispatch(peer):
-        remote(
-            disp.at[slot_rows(0)],
-            xs.at[y, c, slot_rows(peer)],
-            a_send.at[peer],
-            a_recv.at[peer],
-            z=z,
-            x=x,
-        ).wait_recv()
+                key_copy(from_z, r, z).wait_recv()
+            attend(kvb.at[from_z, 0], kvb.at[from_z, 1], False)
+
+    def wait_rows(block, j, recv_sems):
+        k = nearby(j)
+        count = per_chunk - 1 if j == 0 else per_chunk
+        span = pl.ds(pl.multiple_of(k * chunk, chunk), count * cap)
+        wait_arrived(xs.at[block, c, span], recv_sems.at[k])
 
     def chunk_rows(k):
         return pl.ds(pl.multiple_of(k * chunk, chunk), chunk)
@@ -478,22 +518,22 @@
     def up_copy(s, k):
         where = chunk_rows(k)
         block = xs.at[y_at(-s), c, where]
-        return remote(block, block, up_send.at[k, s], up_recv.at[k, s], y=y_next)
+        return remote(block, block, up_send.at[0], up_recv.at[k, s], y=y_next)
 
     def dn_copy(s, k):
         where = chunk_rows(k)
         block = xs.at[y_at(s), c, where]
-        return remote(block, block, dn_send.at[k, s], dn_recv.at[k, s], y=y_prev)
+        return remote(block, block, dn_send.at[0], dn_recv.at[k, s], y=y_prev)
 
     def up_arrival(s, k):
         where = chunk_rows(k)
         block = xs.at[y_at(-s - 1), c, where]
-        return remote(block, block, up_send.at[k, s], up_recv.at[k, s], y=y_next)
+        return remote(block, block, up_send.at[0], up_recv.at[k, s], y=y_next)
 
     def dn_arrival(s, k):
         where = chunk_rows(k)
         block = xs.at[y_at(s + 1), c, where]
-        return remote(block, block, dn_send.at[k, s], dn_recv.at[k, s], y=y_prev)
+        return remote(block, block, dn_send.at[0], dn_recv.at[k, s], y=y_prev)
 
     def mate_block(number, k, core):
         shift = (0, -1, 1, -2, 2, -3, 3, half_ring)[number]
@@ -501,14 +541,11 @@
 
     def mate_copy(number, k):
         block = mate_block(number, k, c)
-        return remote(block, block, m_send.at[k, number], m_recv.at[k, number], c=other)
-
-    def mate_arrival(number, k):
-        block = mate_block(number, k, other)
-        return remote(block, block, m_send.at[k, number], m_recv.at[k, number], c=other)
-
-    def first_sends(k):
-        each_other(k * per_chunk, per_chunk, wait_dispatch)
+        return remote(block, block, m_send.at[0], m_recv.at[k], c=other)
+
+    def first_sends(j):
+        wait_rows(y, j, a_recv)
+        k = nearby(j)
         up_copy(0, k).start()
         dn_copy(0, k).start()
         mate_copy(0, k).start()
@@ -523,32 +560,15 @@
             dn_copy(s + 1, k).start()
         mate_copy(2 * s + 2, k).start()
 
-    def far_rows(k):
-        def wait_far(peer):
-            remote(
-                disp_far.at[slot_rows(0)],
-                xs.at[y_far, c, slot_rows(peer)],
-                f_send.at[peer],
-                f_recv.at[peer],
-                z=z,
-                x=x,
-            ).wait_recv()
-
-        each_other(k * per_chunk, per_chunk, wait_far)
-        mate_copy(ny - 1, k).start()
+    def far_rows(j):
+        wait_rows(y_far, j, f_recv)
+        mate_copy(ny - 1, nearby(j)).start()
 
     def result_copies(r):
         to_x = lax.rem(x + r, nx)
         return (
-            remote(o_out.at[to_x], o_in.at[x], o_send.at[r], o_recv.at[r], x=to_x),
-            remote(stat.at[to_x], stat_in.at[x], s_send.at[r], s_recv.at[r], x=to_x),
-        )
-
-    def result_arrivals(r):
-        from_x = lax.rem(x + nx - r, nx)
-        return (
-            remote(o_out.at[0], o_in.at[from_x], o_send.at[r], o_recv.at[r], x=x),
-            remote(stat.at[0], stat_in.at[from_x], s_send.at[r], s_recv.at[r], x=x),
+            remote(o_out.at[to_x], o_in.at[x], o_send.at[0], o_recv.at[0], x=to_x),
+            remote(stat.at[to_x], stat_in.at[x], s_send.at[0], s_recv.at[0], x=to_x),
         )
 
     def send_results():
@@ -560,8 +580,7 @@
         stat_in[x] = stat[x]
 
     def expert(k):
-        for number in range(ny):
-            mate_arrival(number, k).wait_recv()
+        wait_arrived(xs.at[:, other, chunk_rows(k)], m_recv.at[k])
         gate = jnp.zeros((chunk, gw.shape[1]), F32)
         up = jnp.zeros((chunk, gw.shape[1]), F32)
         for block in range(ny):
@@ -580,7 +599,7 @@
         part_copy(k).start()
 
     def part_copy(k):
-        return remote(parts.at[k, other], mate.at[k], pm_send.at[k], pm_recv.at[k], c=other)
+        return remote(parts.at[k, other], mate.at[k], pm_send.at[0], pm_recv.at[k], c=other)
 
     full = slice(0, chunk)
     top = slice(0, half)
@@ -593,14 +612,14 @@
         where = top if d == half_ring else full
         return remote(
             sb_up.at[k, d - 1, where], rb_up.at[k, d - 1, where],
-            ru_send.at[k, d - 1], ru_recv.at[k, d - 1], y=y_next,
+            ru_send.at[d // half_ring], ru_recv.at[k, d - 1], y=y_next,
         )
 
     def sum_dn(k, d):
         where = bottom if d == half_ring else full
         return remote(
             sb_dn.at[k, d - 1, where], rb_dn.at[k, d - 1, where],
-            rd_send.at[k, d - 1], rd_recv.at[k, d - 1], y=y_prev,
+            rd_send.at[d // half_ring], rd_recv.at[k, d - 1], y=y_prev,
         )
 
     def sum_step(k, d):
@@ -645,8 +664,8 @@
         return remote(
             ans.at[slot_rows(target)],
             ret.at[slot_rows(e)],
-            b_send.at[target],
-            b_recv.at[e],
+            b_send.at[0],
+            b_recv.at[0],
             z=target // nx,
             x=lax.rem(target, nx),
         )
@@ -662,12 +681,12 @@
     def head_up(s, hop):
         where = top_rows if s == half_ring - 1 else all_rows
         block = heads.at[y_at(-s - hop), c, where]
-        return remote(block, block, hu_send.at[s], hu_recv.at[s], y=y_next)
+        return remote(block, block, hu_send.at[(s + 1) // half_ring], hu_recv.at[s], y=y_next)
 
     def head_dn(s, hop):
         where = low_rows if s == half_ring - 1 else all_rows
         block = heads.at[y_at(s + hop), c, where]
-        return remote(block, block, hd_send.at[s], hd_recv.at[s], y=y_prev)
+        return remote(block, block, hd_send.at[(s + 1) // half_ring], hd_recv.at[s], y=y_prev)
 
     def head_mate(number, core):
         s = (number - 1) // 2
@@ -678,7 +697,7 @@
             block = heads.at[y_at(-s - 1), core, top_rows if last else all_rows]
         else:
             block = heads.at[y_at(s + 1), core, low_rows if last else all_rows]
-        return remote(block, block, hm_send.at[number], hm_recv.at[number], c=other)
+        return remote(block, block, hm_send.at[0], hm_recv.at[0], c=other)
 
     def head_pass(s):
         head_up(s, 1).wait_recv()
@@ -691,9 +710,8 @@
         head_mate(2 * s + 2, c).start()
 
     def merge():
-        for r in range(1, nx):
-            for copy in result_arrivals(r):
-                copy.wait_recv()
+        wait_arrived(o_in.at[pl.ds(0, nx - 1)], o_recv.at[0])
+        wait_arrived(stat_in.at[pl.ds(0, nx - 1)], s_recv.at[0])
         top_max = stat_in[0, 0:1, :]
         for j in range(1, nx):
             top_max = jnp.maximum(top_max, stat_in[j, 0:1, :])
@@ -727,18 +745,18 @@
         else:
             answer(k)
 
-    def gather_stage(s, k):
+    def gather_stage(s, j):
         if s == 0:
-            first_sends(k)
+            first_sends(j)
         else:
-            pass_on(s - 1, k)
+            pass_on(s - 1, nearby(j))
 
     weights_here = []
     stages = {
-        "gather": lambda s, j: gather_stage(s, nearby(j)),
+        "gather": gather_stage,
         "inputs": send_inputs,
         "keys": send_far_keys,
-        "far": lambda j: far_rows(nearby(j)),
+        "far": far_rows,
         "chain": chain_step,
         "own": own_attention,
         "attend": attend_far,
@@ -754,8 +772,7 @@
     ret[slot_rows(e), :] = ans[slot_rows(e), :]
 
     weight_copies[3].wait()
-    for number in range(2 * half_ring + 1):
-        head_mate(number, other).wait_recv()
+    wait_arrived(heads.at[:, other], hm_recv.at[0])
     mixed = jnp.zeros((rows, LANES), F32)
     for block in range(ny):
         both = jnp.concatenate([heads[block, 0], heads[block, 1]], axis=1)
@@ -764,59 +781,39 @@
         )
     out_ref[0] = mixed.astype(BF16)
 
-    def drain(peer):
-        dispatch(peer).wait_send()
-        dispatch_far(peer).wait_send()
-
-    each_other(0, nep, drain)
-
-    def drain_chunk(k):
-        for s in range(half_ring - 1):
-            up_copy(s, k).wait_send()
-            dn_copy(s, k).wait_send()
-        for d in range(1, half_ring + 1):
-            sum_up(k, d).wait_send()
-            sum_dn(k, d).wait_send()
-        for number in range(ny):
-            mate_copy(number, k).wait_send()
-        part_copy(k).wait_send()
-
-    loop(0, CHUNKS, drain_chunk)
-    for r in range(1, nx):
-        query_copy(r).wait_send()
-        for copy in result_copies(r):
-            copy.wait_send()
+    others = pl.ds(0, (nep - 1) * cap)
+    wait_sent(disp.at[others], a_send.at[0])
+    wait_sent(disp_far.at[others], f_send.at[0])
+    wait_sent(xs.at[pl.ds(0, half_ring - 1), c], up_send.at[0])
+    wait_sent(xs.at[pl.ds(0, half_ring - 1), c], dn_send.at[0])
+    wait_sent(xs.at[:, c], m_send.at[0])
+    wait_sent(mate, pm_send.at[0])
+    wait_sent(sb_up.at[:, pl.ds(0, half_ring - 1)], ru_send.at[0])
+    wait_sent(sb_up.at[:, half_ring - 1, top], ru_send.at[1])
+    wait_sent(sb_dn.at[:, pl.ds(0, half_ring - 1)], rd_send.at[0])
+    wait_sent(sb_dn.at[:, half_ring - 1, bottom], rd_send.at[1])
+    wait_sent(qb.at[pl.ds(0, nx - 1)], q_send.at[0])
+    wait_sent(o_out.at[pl.ds(0, nx - 1)], o_send.at[0])
+    wait_sent(stat.at[pl.ds(0, nx - 1)], s_send.at[0])
     for r in range(1, reach + 1):
 
         @pl.when((z + 1 < nz) & (z - r + 1 >= 0))
         def _(r=r):
-            for copy in chain_copies(r):
-                copy.wait_send()
+            chain_copy(r).wait_send()
 
     for r in range(reach + 1, nz):
 
         @pl.when(z + r < nz)
         def _(r=r):
-            for copy in far_copies(r):
-                copy.wait_send()
-
-    for s in range(half_ring):
-        head_up(s, 0).wait_send()
-        head_dn(s, 0).wait_send()
-    for number in range(2 * half_ring + 1):
-        head_mate(number, c).wait_send()
-
-    def wait_back(peer):
-        remote(
-            ans.at[slot_rows(0)],
-            ret.at[slot_rows(peer)],
-            b_send.at[peer],
-            b_recv.at[peer],
-            z=z,
-            x=x,
-        ).wait_recv()
-
-    each_other(0, nep, wait_back)
+            far_copy(r).wait_send()
+
+    wait_sent(heads.at[pl.ds(0, half_ring - 1), c], hu_send.at[0])
+    wait_sent(heads.at[0, c, top_rows], hu_send.at[1])
+    wait_sent(heads.at[pl.ds(0, half_ring - 1), c], hd_send.at[0])
+    wait_sent(heads.at[0, c, low_rows], hd_send.at[1])
+    wait_sent(heads.at[:, c], hm_send.at[0])
+
+    wait_arrived(ret.at[pl.ds(0, (nep - 1) * cap)], b_recv.at[0])
     routed = jnp.zeros((LANES, rows), F32)
     for i in range(2):
         routed += weight[i : i + 1, :] * lax.dot_general(
@@ -824,7 +821,7 @@
         )
     out_ref[1] = routed.T.astype(BF16)
 
-    each_other(0, nep, lambda peer: back_copy(peer).wait_send())
+    wait_sent(ans.at[pl.ds(0, (nep - 1) * cap)], b_send.at[0])
 
 
 def local(
@@ -853,7 +850,6 @@
     total = nep * cap
     chunk = total // CHUNKS
     half_ring = ny // 2
-    mates = 2 * half_ring + 1
     dma = pltpu.SemaphoreType.DMA
     vmem = pltpu.VMEM
     scratch = [
@@ -883,50 +879,47 @@
         vmem((CHUNKS, half_ring, chunk, LANES), BF16),
         vmem((total, LANES), BF16),
         vmem((total, LANES), BF16),
-        dma((nep,)),
-        dma((nep,)),
-        dma((nep,)),
-        dma((nep,)),
+        dma((1,)),
+        dma((CHUNKS,)),
+        dma((1,)),
+        dma((CHUNKS,)),
+        dma((1,)),
+        dma((CHUNKS, half_ring - 1)),
+        dma((1,)),
+        dma((CHUNKS, half_ring - 1)),
+        dma((1,)),
+        dma((CHUNKS,)),
+        dma((1,)),
+        dma((CHUNKS,)),
+        dma((2,)),
         dma((CHUNKS, half_ring)),
+        dma((2,)),
         dma((CHUNKS, half_ring)),
-        dma((CHUNKS, half_ring)),
-        dma((CHUNKS, half_ring)),
-        dma((CHUNKS, mates)),
-        dma((CHUNKS, mates)),
-        dma((CHUNKS,)),
-        dma((CHUNKS,)),
-        dma((CHUNKS, half_ring)),
-        dma((CHUNKS, half_ring)),
-        dma((CHUNKS, half_ring)),
-        dma((CHUNKS, half_ring)),
-        dma((nep,)),
-        dma((nep,)),
+        dma((1,)),
+        dma((1,)),
         vmem((nx, rows, LANES), BF16),
         vmem((nx, 2 * rows, LANES), BF16),
-        vmem((nz, rows, LANES), BF16),
-        vmem((nz, rows, LANES), BF16),
+        vmem((nz, 2, rows, LANES), BF16),
         vmem((nx, LANES, 2 * rows), F32),
         vmem((nx, 8, 2 * rows), F32),
         vmem((nx, LANES, 2 * rows), BF16),
         vmem((nx, LANES, 2 * rows), BF16),
         vmem((nx, 8, 2 * rows), F32),
         vmem((ny, 2, rows, LANES), BF16),
-        dma((nx,)),
-        dma((nx,)),
+        dma((1,)),
+        dma((1,)),
         dma((nz,)),
         dma((nz,)),
-        dma((nz,)),
-        dma((nz,)),
-        dma((nx,)),
-        dma((nx,)),
-        dma((nx,)),
-        dma((nx,)),
+        dma((1,)),
+        dma((1,)),
+        dma((1,)),
+        dma((1,)),
+        dma((2,)),
         dma((half_ring,)),
+        dma((2,)),
         dma((half_ring,)),
-        dma((half_ring,)),
-        dma((half_ring,)),
-        dma((mates,)),
-        dma((mates,)),
+        dma((1,)),
+        dma((1,)),
     ]
     whole = pl.BlockSpec(memory_space=pltpu.VMEM)
     far = pl.BlockSpec(memory_space=pl.ANY)

time: 83.9 us -> 79.7 us (0.950)
  Pallas kernels: 80.8 us -> 76.7 us
    pallas_call x1, Pallas kernels: 80.8 us -> 76.7 us  [local(): pl.pallas_call(lambda *refs: kernel(sizes, *refs), out_shape=jax.ShapeDty...]
where the time goes in v6:
time: 79.7 us; the launch traced here: 79.5 us
  Pallas kernels  76.7 us (96%)
  local copies, waits for them, and re-layouts  1.53 us (2%)
  between operations  1.29 us (2%)
    pallas_call x1, Pallas kernels, local(): pl.pallas_call(lambda *refs: kernel(sizes, *refs), out_shape=jax.ShapeDty...  76.7 us

profile of v6, /device:TPU:1, one launch (start us, length us, event | category | flops | bytes accessed | tf_op | source)
XLA Modules:
  0.0 79.5 jit_solution(9515293376006593104)
XLA Ops:
  1.3 76.7 %shard_map.149 = bf16[2,256,128]{2,1,0:T(8,128)(2,1)} custom-call(bf16[256,128]{1,0:T(8,128)(2,1)} %refs_0_.1, bf16[256,128]{1,0:T(8,128)(2,1)} %refs_1_.1, bf16[256,128]{1,0:T(8,128)(2,1)} %refs_2_.1, f32[1,1]{1,0:T(1,128)} %bitcast.13.refs_3_, f32[1,128]{1,0:T(1,128)} %bitcast.21, bf16[2048,128]{1,0:T(8,128)(2,1)} %refs_5_.1, bf16[256,2048]{1,0:T(8,128)(2,1)} %refs_6_.1, ...), custom_call_target="tpu_custom_call" | custom-call | tf_op jit(solution)/shard_map/pallas_call | solution.py:926
  78.0 1.5 %slice_bitcast_fusion = (bf16[256,128]{1,0:T(8,128)(2,1)}, bf16[256,128]{1,0:T(8,128)(2,1)}) fusion(bf16[2,256,128]{2,1,0:T(8,128)(2,1)} %shard_map.149), kind=kLoop, calls=%fused_computation | loop fusion | bytes 262144 | tf_op jit(solution)/shard_map/squeeze | solution.py:951

commit v7 on v6

--- a/solution.py
+++ b/solution.py
@@ -119,8 +119,9 @@
     ("sum", 0, 5),
     ("sum", 0, 6),
     ("heads", 3),
+    ("drain",),
+    ("project",),
     ("heads", 4),
-    ("project",),
 )
 F32 = jnp.float32
 BF16 = jnp.bfloat16
@@ -192,18 +193,14 @@
     a_recv,
     f_send,
     f_recv,
-    up_send,
-    up_recv,
-    dn_send,
-    dn_recv,
+    g_send,
+    g_recv,
     m_send,
     m_recv,
     pm_send,
     pm_recv,
-    ru_send,
-    ru_recv,
-    rd_send,
-    rd_recv,
+    r_send,
+    r_recv,
     b_send,
     b_recv,
     qb,
@@ -215,6 +212,7 @@
     o_in,
     stat_in,
     heads,
+    mixed,
     q_send,
     q_recv,
     k_send,
@@ -223,10 +221,8 @@
     o_recv,
     s_send,
     s_recv,
-    hu_send,
-    hu_recv,
-    hd_send,
-    hd_recv,
+    h_send,
+    h_recv,
     hm_send,
     hm_recv,
 ):
@@ -518,22 +514,12 @@
     def up_copy(s, k):
         where = chunk_rows(k)
         block = xs.at[y_at(-s), c, where]
-        return remote(block, block, up_send.at[0], up_recv.at[k, s], y=y_next)
+        return remote(block, block, g_send.at[0], g_recv.at[0, k, s], y=y_next)
 
     def dn_copy(s, k):
         where = chunk_rows(k)
         block = xs.at[y_at(s), c, where]
-        return remote(block, block, dn_send.at[0], dn_recv.at[k, s], y=y_prev)
-
-    def up_arrival(s, k):
-        where = chunk_rows(k)
-        block = xs.at[y_at(-s - 1), c, where]
-        return remote(block, block, up_send.at[0], up_recv.at[k, s], y=y_next)
-
-    def dn_arrival(s, k):
-        where = chunk_rows(k)
-        block = xs.at[y_at(s + 1), c, where]
-        return remote(block, block, dn_send.at[0], dn_recv.at[k, s], y=y_prev)
+        return remote(block, block, g_send.at[0], g_recv.at[1, k, s], y=y_prev)
 
     def mate_block(number, k, core):
         shift = (0, -1, 1, -2, 2, -3, 3, half_ring)[number]
@@ -551,11 +537,11 @@
         mate_copy(0, k).start()
 
     def pass_on(s, k):
-        up_arrival(s, k).wait_recv()
+        wait_arrived(xs.at[y_at(-s - 1), c, chunk_rows(k)], g_recv.at[0, k, s])
         if s + 2 < half_ring:
             up_copy(s + 1, k).start()
         mate_copy(2 * s + 1, k).start()
-        dn_arrival(s, k).wait_recv()
+        wait_arrived(xs.at[y_at(s + 1), c, chunk_rows(k)], g_recv.at[1, k, s])
         if s + 2 < half_ring:
             dn_copy(s + 1, k).start()
         mate_copy(2 * s + 2, k).start()
@@ -612,14 +598,14 @@
         where = top if d == half_ring else full
         return remote(
             sb_up.at[k, d - 1, where], rb_up.at[k, d - 1, where],
-            ru_send.at[d // half_ring], ru_recv.at[k, d - 1], y=y_next,
+            r_send.at[d // half_ring], r_recv.at[0, k, d - 1], y=y_next,
         )
 
     def sum_dn(k, d):
         where = bottom if d == half_ring else full
         return remote(
             sb_dn.at[k, d - 1, where], rb_dn.at[k, d - 1, where],
-            rd_send.at[d // half_ring], rd_recv.at[k, d - 1], y=y_prev,
+            r_send.at[d // half_ring], r_recv.at[1, k, d - 1], y=y_prev,
         )
 
     def sum_step(k, d):
@@ -678,15 +664,15 @@
     low_rows = pl.ds(rows // 2, rows // 2)
     all_rows = pl.ds(0, rows)
 
-    def head_up(s, hop):
+    def head_up(s):
         where = top_rows if s == half_ring - 1 else all_rows
-        block = heads.at[y_at(-s - hop), c, where]
-        return remote(block, block, hu_send.at[(s + 1) // half_ring], hu_recv.at[s], y=y_next)
-
-    def head_dn(s, hop):
+        block = heads.at[y_at(-s), c, where]
+        return remote(block, block, h_send.at[(s + 1) // half_ring], h_recv.at[0, s], y=y_next)
+
+    def head_dn(s):
         where = low_rows if s == half_ring - 1 else all_rows
-        block = heads.at[y_at(s + hop), c, where]
-        return remote(block, block, hd_send.at[(s + 1) // half_ring], hd_recv.at[s], y=y_prev)
+        block = heads.at[y_at(s), c, where]
+        return remote(block, block, h_send.at[(s + 1) // half_ring], h_recv.at[1, s], y=y_prev)
 
     def head_mate(number, core):
         s = (number - 1) // 2
@@ -697,16 +683,17 @@
             block = heads.at[y_at(-s - 1), core, top_rows if last else all_rows]
         else:
             block = heads.at[y_at(s + 1), core, low_rows if last else all_rows]
-        return remote(block, block, hm_send.at[0], hm_recv.at[0], c=other)
+        return remote(block, block, hm_send.at[0], hm_recv.at[1 if last else 0], c=other)
 
     def head_pass(s):
-        head_up(s, 1).wait_recv()
-        if s + 1 < half_ring:
-            head_up(s + 1, 0).start()
+        last = s == half_ring - 1
+        wait_arrived(heads.at[y_at(-s - 1), c, top_rows if last else all_rows], h_recv.at[0, s])
+        if not last:
+            head_up(s + 1).start()
         head_mate(2 * s + 1, c).start()
-        head_dn(s, 1).wait_recv()
-        if s + 1 < half_ring:
-            head_dn(s + 1, 0).start()
+        wait_arrived(heads.at[y_at(s + 1), c, low_rows if last else all_rows], h_recv.at[1, s])
+        if not last:
+            head_dn(s + 1).start()
         head_mate(2 * s + 2, c).start()
 
     def merge():
@@ -726,8 +713,8 @@
         mean = jnp.sum(difference * difference, axis=0, keepdims=True) * (1.0 / LANES)
         head = difference * lax.rsqrt(mean + EPSILON)
         heads[y, c] = (head.T * hgain_ref[...]).astype(BF16)
-        head_up(0, 0).start()
-        head_dn(0, 0).start()
+        head_up(0).start()
+        head_dn(0).start()
         head_mate(0, c).start()
 
     def weights_and_expert(k):
@@ -750,6 +737,43 @@
             first_sends(j)
         else:
             pass_on(s - 1, nearby(j))
+
+    def project_block(block):
+        both = jnp.concatenate([heads[block, 0], heads[block, 1]], axis=1)
+        depth = pl.ds(pl.multiple_of(block * 2 * LANES, 2 * LANES), 2 * LANES)
+        return jnp.dot(both, ow[depth, :], preferred_element_type=F32)
+
+    def project_most():
+        weight_copies[3].wait()
+        wait_arrived(heads.at[pl.ds(0, ny - 1), other], hm_recv.at[0])
+        total_so_far = project_block(y)
+        for shift in range(1, half_ring):
+            total_so_far += project_block(y_at(shift)) + project_block(y_at(-shift))
+        mixed[...] = total_so_far
+
+    def drain():
+        others = pl.ds(0, (nep - 1) * cap)
+        wait_sent(disp.at[others], a_send.at[0])
+        wait_sent(disp_far.at[others], f_send.at[0])
+        wait_sent(xs.at[pl.ds(0, 2 * half_ring - 2), c], g_send.at[0])
+        wait_sent(xs.at[:, c], m_send.at[0])
+        wait_sent(mate, pm_send.at[0])
+        wait_sent(mate.at[:, pl.ds(0, 2 * half_ring - 2)], r_send.at[0])
+        wait_sent(sb_up.at[:, 0], r_send.at[1])
+        wait_sent(qb.at[pl.ds(0, nx - 1)], q_send.at[0])
+        wait_sent(o_out.at[pl.ds(0, nx - 1)], o_send.at[0])
+        wait_sent(stat.at[pl.ds(0, nx - 1)], s_send.at[0])
+        for r in range(1, reach + 1):
+
+            @pl.when((z + 1 < nz) & (z - r + 1 >= 0))
+            def _(r=r):
+                chain_copy(r).wait_send()
+
+        for r in range(reach + 1, nz):
+
+            @pl.when(z + r < nz)
+            def _(r=r):
+                far_copy(r).wait_send()
 
     weights_here = []
     stages = {
@@ -765,52 +789,18 @@
         "results": send_results,
         "merge": merge,
         "heads": lambda s: head_pass(s - 1),
-        "project": lambda: None,
+        "drain": drain,
+        "project": project_most,
     }
     for stage in ORDER:
         stages[stage[0]](*stage[1:])
     ret[slot_rows(e), :] = ans[slot_rows(e), :]
 
-    weight_copies[3].wait()
-    wait_arrived(heads.at[:, other], hm_recv.at[0])
-    mixed = jnp.zeros((rows, LANES), F32)
-    for block in range(ny):
-        both = jnp.concatenate([heads[block, 0], heads[block, 1]], axis=1)
-        mixed += jnp.dot(
-            both, ow[block * 2 * LANES : (block + 1) * 2 * LANES, :], preferred_element_type=F32
-        )
-    out_ref[0] = mixed.astype(BF16)
-
-    others = pl.ds(0, (nep - 1) * cap)
-    wait_sent(disp.at[others], a_send.at[0])
-    wait_sent(disp_far.at[others], f_send.at[0])
-    wait_sent(xs.at[pl.ds(0, half_ring - 1), c], up_send.at[0])
-    wait_sent(xs.at[pl.ds(0, half_ring - 1), c], dn_send.at[0])
-    wait_sent(xs.at[:, c], m_send.at[0])
-    wait_sent(mate, pm_send.at[0])
-    wait_sent(sb_up.at[:, pl.ds(0, half_ring - 1)], ru_send.at[0])
-    wait_sent(sb_up.at[:, half_ring - 1, top], ru_send.at[1])
-    wait_sent(sb_dn.at[:, pl.ds(0, half_ring - 1)], rd_send.at[0])
-    wait_sent(sb_dn.at[:, half_ring - 1, bottom], rd_send.at[1])
-    wait_sent(qb.at[pl.ds(0, nx - 1)], q_send.at[0])
-    wait_sent(o_out.at[pl.ds(0, nx - 1)], o_send.at[0])
-    wait_sent(stat.at[pl.ds(0, nx - 1)], s_send.at[0])
-    for r in range(1, reach + 1):
-
-        @pl.when((z + 1 < nz) & (z - r + 1 >= 0))
-        def _(r=r):
-            chain_copy(r).wait_send()
-
-    for r in range(reach + 1, nz):
-
-        @pl.when(z + r < nz)
-        def _(r=r):
-            far_copy(r).wait_send()
-
-    wait_sent(heads.at[pl.ds(0, half_ring - 1), c], hu_send.at[0])
-    wait_sent(heads.at[0, c, top_rows], hu_send.at[1])
-    wait_sent(heads.at[pl.ds(0, half_ring - 1), c], hd_send.at[0])
-    wait_sent(heads.at[0, c, low_rows], hd_send.at[1])
+    wait_arrived(heads.at[0, other], hm_recv.at[1])
+    out_ref[0] = (mixed[...] + project_block(y_far)).astype(BF16)
+
+    wait_sent(heads.at[pl.ds(0, 2 * half_ring - 2), c], h_send.at[0])
+    wait_sent(heads.at[0, c], h_send.at[1])
     wait_sent(heads.at[:, c], hm_send.at[0])
 
     wait_arrived(ret.at[pl.ds(0, (nep - 1) * cap)], b_recv.at[0])
@@ -884,17 +874,13 @@
         dma((1,)),
         dma((CHUNKS,)),
         dma((1,)),
-        dma((CHUNKS, half_ring - 1)),
-        dma((1,)),
-        dma((CHUNKS, half_ring - 1)),
+        dma((2, CHUNKS, half_ring - 1)),
         dma((1,)),
         dma((CHUNKS,)),
         dma((1,)),
         dma((CHUNKS,)),
         dma((2,)),
-        dma((CHUNKS, half_ring)),
-        dma((2,)),
-        dma((CHUNKS, half_ring)),
+        dma((2, CHUNKS, half_ring)),
         dma((1,)),
         dma((1,)),
         vmem((nx, rows, LANES), BF16),
@@ -906,6 +892,7 @@
         vmem((nx, LANES, 2 * rows), BF16),
         vmem((nx, 8, 2 * rows), F32),
         vmem((ny, 2, rows, LANES), BF16),
+        vmem((rows, LANES), F32),
         dma((1,)),
         dma((1,)),
         dma((nz,)),
@@ -915,17 +902,15 @@
         dma((1,)),
         dma((1,)),
         dma((2,)),
-        dma((half_ring,)),
+        dma((2, half_ring)),
+        dma((1,)),
         dma((2,)),
-        dma((half_ring,)),
-        dma((1,)),
-        dma((1,)),
     ]
     whole = pl.BlockSpec(memory_space=pltpu.VMEM)
     far = pl.BlockSpec(memory_space=pl.ANY)
     both = pl.pallas_call(
         lambda *refs: kernel(sizes, *refs),
-        out_shape=jax.ShapeDtypeStruct((2, rows, LANES), BF16),
+        out_shape=pltpu.VMEM((2, rows, LANES), BF16),
         in_specs=[far] * 14,
         out_specs=whole,
         scratch_shapes=scratch,

time: 79.7 us -> 77.9 us (0.977)
  Pallas kernels: 76.7 us -> 75.8 us
  local copies, waits for them, and re-layouts: 1.53 us -> 0.66 us
    squeeze x1, local copies, waits for them, and re-layouts: 1.53 us -> 0.66 us  [local(): return (both[0], both[1])]
    pallas_call x1, Pallas kernels: 76.7 us -> 75.8 us  [local(): pl.pallas_call(lambda *refs: kernel(sizes, *refs), out_shape=pltpu.VMEM((...]
where the time goes in v7:
time: 77.9 us; the launch traced here: 77.8 us
  Pallas kernels  75.8 us (97%)
  between operations  1.29 us (2%)
    pallas_call x1, Pallas kernels, local(): pl.pallas_call(lambda *refs: kernel(sizes, *refs), out_shape=pltpu.VMEM((...  75.8 us

profile of v7, /device:TPU:1, one launch (start us, length us, event | category | flops | bytes accessed | tf_op | source)
XLA Modules:
  0.0 77.8 jit_solution(6420632156575319087)
XLA Ops:
  1.3 75.8 %shard_map.149 = bf16[2,256,128]{2,1,0:T(8,128)(2,1)S(1)} custom-call(bf16[256,128]{1,0:T(8,128)(2,1)} %refs_0_.1, bf16[256,128]{1,0:T(8,128)(2,1)} %refs_1_.1, bf16[256,128]{1,0:T(8,128)(2,1)} %refs_2_.1, f32[1,1]{1,0:T(1,128)} %bitcast.13.refs_3_, f32[1,128]{1,0:T(1,128)} %bitcast.21, bf16[2048,128]{1,0:T(8,128)(2,1)} %refs_5_.1, ...), custom_call_target="tpu_custom_call" | custom-call | tf_op jit(solution)/shard_map/pallas_call | solution.py:911
  77.1 0.7 slice_bitcast_fusion

commit v8 on v7

--- a/solution.py
+++ b/solution.py
@@ -456,6 +456,7 @@
             if number + 1 < len(pieces):
                 ahead = score(*pieces[number + 1])
             columns = slice(first, first + LANES)
+            sums_at = slice(maps + first, maps + first + LANES)
             if masked:
                 key_pos = x * rows + lax.broadcasted_iota(jnp.int32, scores.shape, 0)
                 query_pos = lax.broadcasted_iota(jnp.int32, scores.shape, 1) + (
@@ -473,10 +474,10 @@
             total_terms = jnp.sum(terms, axis=0, keepdims=True)
             weighted = jnp.dot(values, terms.astype(BF16), preferred_element_type=F32)
             if masked:
-                stat[index, 1:2, columns] = total_terms
+                stat[index, 0:1, sums_at] = total_terms
                 acc[index, :, columns] = weighted
             else:
-                stat[index, 1:2, columns] = stat[index, 1:2, columns] * factor + total_terms
+                stat[index, 0:1, sums_at] = stat[index, 0:1, sums_at] * factor + total_terms
                 acc[index, :, columns] = acc[index, :, columns] * factor + weighted
             stat[index, 0:1, columns] = new_max
 
@@ -699,14 +700,14 @@
     def merge():
         wait_arrived(o_in.at[pl.ds(0, nx - 1)], o_recv.at[0])
         wait_arrived(stat_in.at[pl.ds(0, nx - 1)], s_recv.at[0])
-        top_max = stat_in[0, 0:1, :]
+        top_max = stat_in[0, 0:1, :maps]
         for j in range(1, nx):
-            top_max = jnp.maximum(top_max, stat_in[j, 0:1, :])
+            top_max = jnp.maximum(top_max, stat_in[j, 0:1, :maps])
         denominator = jnp.zeros_like(top_max)
         weighted = jnp.zeros(o_in.shape[1:], F32)
         for j in range(nx):
-            factor = jnp.exp(stat_in[j, 0:1, :] - top_max)
-            denominator += factor * stat_in[j, 1:2, :]
+            factor = jnp.exp(stat_in[j, 0:1, :maps] - top_max)
+            denominator += factor * stat_in[j, 0:1, maps:]
             weighted += factor * o_in[j].astype(F32)
         mapped = weighted / denominator
         difference = mapped[:, :rows] - scale_ref[0:1, 0:1] * mapped[:, rows:]
@@ -887,10 +888,10 @@
         vmem((nx, 2 * rows, LANES), BF16),
         vmem((nz, 2, rows, LANES), BF16),
         vmem((nx, LANES, 2 * rows), F32),
-        vmem((nx, 8, 2 * rows), F32),
+        vmem((nx, 1, 4 * rows), F32),
         vmem((nx, LANES, 2 * rows), BF16),
         vmem((nx, LANES, 2 * rows), BF16),
-        vmem((nx, 8, 2 * rows), F32),
+        vmem((nx, 1, 4 * rows), F32),
         vmem((ny, 2, rows, LANES), BF16),
         vmem((rows, LANES), F32),
         dma((1,)),

time: 77.9 us -> 77.4 us (level)
  no operation moved by 1% of the time
where the time goes in v8:
time: 77.4 us; the launch traced here: 77.2 us
  Pallas kernels  75.3 us (97%)
  between operations  1.29 us (2%)
    pallas_call x1, Pallas kernels, local(): pl.pallas_call(lambda *refs: kernel(sizes, *refs), out_shape=pltpu.VMEM((...  75.3 us

profile of v8, /device:TPU:1, one launch (start us, length us, event | category | flops | bytes accessed | tf_op | source)
XLA Modules:
  0.0 77.2 jit_solution(13894140475578327858)
XLA Ops:
  1.3 75.3 %shard_map.149 = bf16[2,256,128]{2,1,0:T(8,128)(2,1)S(1)} custom-call(bf16[256,128]{1,0:T(8,128)(2,1)} %refs_0_.1, bf16[256,128]{1,0:T(8,128)(2,1)} %refs_1_.1, bf16[256,128]{1,0:T(8,128)(2,1)} %refs_2_.1, f32[1,1]{1,0:T(1,128)} %bitcast.13.refs_3_, f32[1,128]{1,0:T(1,128)} %bitcast.21, bf16[2048,128]{1,0:T(8,128)(2,1)} %refs_5_.1, ...), custom_call_target="tpu_custom_call" | custom-call | tf_op jit(solution)/shard_map/pallas_call | solution.py:912
  76.6 0.7 slice_bitcast_fusion
